TPU v7x, 32 devices: a whole 2x2x4 slice. The times are simulated.
32 devices in a mesh: sp: 8 (over z, x), tp: 4 (over y, core).
Axes of the slice: x: 2, y: 2, z: 4, core: 2. Of those that a mesh axis runs over, the one named last changes fastest.
Arguments:
- query_nope: bfloat16 [2048, 1024], P('sp', 'tp'), may hold values from -24 to 24
- query_rope: bfloat16 [2048, 512], P('sp', 'tp'), may hold values from -384 to 384
- latent: bfloat16 [2048, 256], P('sp'), may hold values from -6 to 6
- key_rope: bfloat16 [2048, 64], P('sp'), may hold values from -8 to 8
- latent_gain: bfloat16 [256], replicated, may hold values from 0.099609375 to 1.8984375
- key_up: bfloat16 [256, 1024], replicated, may hold values from -0.375 to 0.375
- value_up: bfloat16 [256, 1024], replicated, may hold values from -0.375 to 0.375
- out_proj: bfloat16 [1024, 2048], P('tp'), may hold values from -0.1875 to 0.1875
- residual: bfloat16 [2048, 2048], P(('sp', 'tp')), may hold values from -6 to 6
- ffn_gain: bfloat16 [2048], replicated, may hold values from 0.099609375 to 1.8984375
- expert_ids: int32 [2048, 4], P(('sp', 'tp')), may hold values from 0 to 7, all different within a row; in each aligned block of 64 rows (0 to 63, 64 to 127, ...) at most 64 rows name the same one
- route_weights: float32 [2048, 4], P(('sp', 'tp')), may hold values from 0.1 to 1
- expert_gate: bfloat16 [8, 2048, 384], P('sp'), may hold values from -0.125 to 0.125
- expert_up: bfloat16 [8, 2048, 384], P('sp'), may hold values from -0.125 to 0.125
- expert_down: bfloat16 [8, 384, 2048], P('sp'), may hold values from -0.3125 to 0.3125
- shared_gate: bfloat16 [2048, 384], replicated, may hold values from -0.125 to 0.125
- shared_up: bfloat16 [2048, 384], replicated, may hold values from -0.125 to 0.125
- shared_down: bfloat16 [384, 2048], replicated, may hold values from -0.3125 to 0.3125
Outputs:
- layer_out: bfloat16 [2048, 2048], P(('sp', 'tp'))
Inputs may be any that keep to these rules, and one draw needn't show every extreme that they name: `expert_ids`: each row names 4 different experts; among the 64 rows of one aligned block no expert is named by more than 64 rows.
All inputs are finite; a program needn't handle non-finite values.
Results may differ from a plain program's by a relative error of at most 0.017.
Values may be sent and summed in bfloat16 or wider, within the bound.
A program may use at most 128 MiB of HBM per device.

v0:
```python
import math

import jax
import jax.numpy as jnp
from jax import lax
from jax.sharding import PartitionSpec as P

NOPE = 128
ROPE = 64
VDIM = 128


rope_base = 10000.0
norm_eps = 1e-06


def scale_rows(values, gain_vec):
    as_float = values.astype(jnp.float32)
    factor = lax.rsqrt(jnp.mean(as_float * as_float, axis=-1, keepdims=True) + norm_eps)
    return (as_float * factor * gain_vec.astype(jnp.float32)).astype(jnp.bfloat16)


def rotate(values, positions):
    half_dim = values.shape[-1] // 2
    frequency = rope_base ** (-jnp.arange(half_dim, dtype=jnp.float32) / half_dim)
    angles = positions.astype(jnp.float32)[:, None, None] * frequency
    cosine = jnp.cos(angles)
    sine_part = jnp.sin(angles)
    as_float = values.astype(jnp.float32)
    first_half = as_float[..., :half_dim]
    second_half = as_float[..., half_dim:]
    return jnp.concatenate(
        [
            first_half * cosine - second_half * sine_part,
            first_half * sine_part + second_half * cosine,
        ],
        axis=-1,
    ).astype(jnp.bfloat16)


def body(
    query_nope,
    query_rope,
    latent,
    key_rope,
    latent_gain,
    key_up,
    value_up,
    out_proj,
    residual,
    ffn_gain,
    expert_ids,
    route_weights,
    expert_gate,
    expert_up,
    expert_down,
    shared_gate,
    shared_up,
    shared_down,
):
    row_count = latent.shape[0]
    first_row = lax.axis_index("sp") * row_count
    last_row = first_row + row_count - 1
    positions = first_row + jnp.arange(row_count, dtype=jnp.int32)
    local_heads = query_nope.shape[1] // NOPE
    head_start = lax.axis_index("tp") * local_heads
    key_local = lax.dynamic_slice_in_dim(key_up, head_start * NOPE, local_heads * NOPE, 1)
    value_local = lax.dynamic_slice_in_dim(value_up, head_start * VDIM, local_heads * VDIM, 1)
    normed_latent = scale_rows(latent, latent_gain)
    rot_key = rotate(key_rope[:, None, :], positions)[:, 0, :]
    queries_nope = query_nope.reshape(row_count, local_heads, NOPE)
    rot_query = rotate(query_rope.reshape(row_count, local_heads, ROPE), positions)
    score_scale = 1.0 / math.sqrt(NOPE + ROPE)

    def expand(block_latent):
        keys_flat = jnp.dot(block_latent, key_local, preferred_element_type=jnp.float32).astype(
            jnp.bfloat16
        )
        values_flat = jnp.dot(block_latent, value_local, preferred_element_type=jnp.float32).astype(
            jnp.bfloat16
        )
        return (keys_flat, values_flat)

    def attend(state_now, keys_flat, values_flat, keys_rope, key_start):
        running, weight_sum, weighted = state_now
        key_count = keys_flat.shape[0]
        key_heads = keys_flat.reshape(key_count, local_heads, NOPE)
        value_heads = values_flat.reshape(key_count, local_heads, VDIM)
        scores = jnp.einsum(
            "qhd,khd->hqk", queries_nope, key_heads, preferred_element_type=jnp.float32
        )
        scores = (
            scores
            + jnp.einsum("qhd,kd->hqk", rot_query, keys_rope, preferred_element_type=jnp.float32)
        ) * score_scale
        key_pos = key_start + jnp.arange(key_count, dtype=jnp.int32)
        allowed = (key_pos[None, :] <= positions[:, None])[None]
        scores = jnp.where(allowed, scores, -1e30)
        newest = jnp.maximum(running, jnp.max(scores, axis=-1))
        weights = jnp.where(allowed, jnp.exp(scores - newest[..., None]), 0.0)
        shrink = jnp.exp(running - newest)
        weight_sum = weight_sum * shrink + jnp.sum(weights, axis=-1)
        mixed = jnp.einsum(
            "hqk,khd->qhd",
            weights.astype(jnp.bfloat16),
            value_heads,
            preferred_element_type=jnp.float32,
        )
        weighted = weighted * shrink.T[:, :, None] + mixed
        return (newest, weight_sum, weighted)

    initial = (
        jnp.full((local_heads, row_count), -jnp.inf, jnp.float32),
        jnp.zeros((local_heads, row_count), jnp.float32),
        jnp.zeros((row_count, local_heads, VDIM), jnp.float32),
    )
    pieces = (
        lax.all_gather(normed_latent, "sp", axis=0, tiled=True),
        lax.all_gather(rot_key, "sp", axis=0, tiled=True),
    )
    piece_len = pieces[0].shape[0]
    span_len = math.gcd(piece_len, 1024)

    def advance(step_num, state_in):
        offset = step_num * span_len
        sliced = tuple((lax.dynamic_slice_in_dim(member, offset, span_len, 0) for member in pieces))

        def compute(state_cur):
            keys_flat, values_flat = expand(sliced[0])
            return attend(state_cur, keys_flat, values_flat, sliced[-1], offset)

        def unchanged(state_cur):
            return state_cur

        return lax.cond(offset <= last_row, compute, unchanged, state_in)

    folded = lax.fori_loop(0, piece_len // span_len, advance, initial)
    heads_out = (
        (folded[2] / folded[1].T[:, :, None])
        .astype(jnp.bfloat16)
        .reshape(row_count, local_heads * VDIM)
    )
    tokens = residual.shape[0]
    attn_sum = lax.psum_scatter(
        jnp.dot(heads_out, out_proj, preferred_element_type=jnp.float32).astype(jnp.bfloat16),
        "tp",
        scatter_dimension=0,
        tiled=True,
    ).astype(jnp.float32)
    hidden_one = (residual.astype(jnp.float32) + attn_sum).astype(jnp.bfloat16)
    normed = scale_rows(hidden_one, ffn_gain)
    slot_count = expert_ids.shape[1]
    model_width = residual.shape[1]
    local_experts = expert_gate.shape[0]
    experts = local_experts * lax.axis_size("sp")
    capacity = max(2, 2 * tokens * slot_count // experts)
    flat_ids = expert_ids.reshape(-1)
    onehot = (flat_ids[:, None] == jnp.arange(experts, dtype=jnp.int32)[None, :]).astype(jnp.int32)
    slot_rank = jnp.sum(jnp.cumsum(onehot, axis=0) * onehot, axis=1) - 1
    target = flat_ids * capacity + slot_rank
    slot_token = (
        jnp.full((experts * capacity,), tokens, jnp.int32)
        .at[target]
        .set(jnp.arange(tokens * slot_count, dtype=jnp.int32) // slot_count)
    )
    padded = jnp.concatenate([normed, jnp.zeros((1, model_width), jnp.bfloat16)], axis=0)
    outgoing = padded[slot_token].reshape(experts, capacity, model_width)
    arrived = lax.all_to_all(outgoing, "sp", split_axis=0, concat_axis=0, tiled=True)
    item_count = arrived.shape[1]
    grouped = arrived.reshape(-1, local_experts, item_count, model_width)
    gate_part = jnp.einsum(
        "seid,edf->seif", grouped, expert_gate, preferred_element_type=jnp.float32
    )
    upper_part = jnp.einsum(
        "seid,edf->seif", grouped, expert_up, preferred_element_type=jnp.float32
    )
    expert_hidden = (jax.nn.silu(gate_part) * upper_part).astype(jnp.bfloat16)
    expert_rows = jnp.einsum(
        "seif,efd->seid", expert_hidden, expert_down, preferred_element_type=jnp.float32
    ).astype(jnp.bfloat16)
    answered = expert_rows.reshape(-1, item_count, model_width)
    returned = lax.all_to_all(answered, "sp", split_axis=0, concat_axis=0, tiled=True)
    picked = returned.reshape(experts * capacity, model_width)[target]
    routed = jnp.sum(
        (picked.astype(jnp.float32) * route_weights.reshape(-1)[:, None]).reshape(
            tokens, slot_count, model_width
        ),
        axis=1,
    ).astype(jnp.bfloat16)
    shared_gate_part = jnp.dot(normed, shared_gate, preferred_element_type=jnp.float32)
    shared_upper = jnp.dot(normed, shared_up, preferred_element_type=jnp.float32)
    shared_hidden = (jax.nn.silu(shared_gate_part) * shared_upper).astype(jnp.bfloat16)
    shared_rows = jnp.dot(shared_hidden, shared_down, preferred_element_type=jnp.float32).astype(
        jnp.bfloat16
    )
    return (
        hidden_one.astype(jnp.float32)
        + routed.astype(jnp.float32)
        + shared_rows.astype(jnp.float32)
    ).astype(jnp.bfloat16)


def solution(mesh):
    in_specs = (
        P("sp", "tp"),
        P("sp", "tp"),
        P("sp", None),
        P("sp", None),
        P(),
        P(),
        P(),
        P("tp", None),
        P(("sp", "tp"), None),
        P(),
        P(("sp", "tp"), None),
        P(("sp", "tp"), None),
        P("sp", None, None),
        P("sp", None, None),
        P("sp", None, None),
        P(),
        P(),
        P(),
    )
    out_specs = P(("sp", "tp"), None)
    return jax.shard_map(body, mesh=mesh, in_specs=in_specs, out_specs=out_specs, check_vma=False)
```

profile of v0, /device:TPU:0, one launch (start us, length us, event | category | flops | bytes accessed | tf_op | source)
XLA Modules:
  0.0 230.2 jit_solution(15625540233846017140)
XLA Ops:
  6.5 1.1 fusion.55
  7.7 0.7 convert_element_type.125
  8.4 1.7 fusion.57
  10.1 0.9 copy.26
  11.0 1.0 copy.25
  12.1 0.1 copy.27
  12.2 0.8 bitcast_convert_fusion
  13.0 0.2 fusion.73
  13.2 0.2 multiply_cosine_fusion
  13.4 33.1 %all_gather.7 = bf16[2048,64]{0,1:T(8,128)(2,1)S(1)} all-gather(bf16[256,64]{0,1:T(8,128)(2,1)S(1)} %pad_maximum_fusion.1), channel_id=1, replica_groups=mesh['sp'=8,'tp'=4] {'sp'}, dimensions={0}, use_global_device_ids=true | all-gather | bytes 294912 | tf_op jit(solution)/shard_map/all_gather | solution.py:119
  46.5 1.0 constant_dynamic-slice_fusion
  47.5 6.6 %all-gather.2.cloned.1.call-done = bf16[2048,256]{1,0:T(8,128)(2,1)} async-done(((bf16[256,256]{1,0:T(8,128)(2,1)}), bf16[2048,256]{1,0:T(8,128)(2,1)}) %all-gather.2.cloned.1.call-update) | async-done | bytes 1048592 | tf_op jit(solution)/shard_map/all_gather | solution.py:118
  54.1 0.7 broadcast_in_dim.64
  54.9 5.2 %while.18 = (s32[]{:T(128)}, f32[2,256]{1,0:T(2,128)S(1)}, f32[2,256]{1,0:T(2,128)S(1)}, f32[256,2,128]{0,2,1:T(8,128)}, s32[]{:T(128)}, /*index=5*/bf16[2048,25...) while((s32[]{:T(128)}, f32[2,256]{1,0:T(2,128)S(1)}, ...), condition=%wide.region_6.7_spmd.clone, body=%wide.region_1.6_spmd.clone.sunk | while | flops 610142976 | bytes 22131136 | solution.py:137
  54.9 5.1 %conditional.3 = ((f32[2,256]{1,0:T(2,128)S(1)}, f32[2,256]{1,0:T(2,128)S(1)}, f32[256,2,128]{0,2,1:T(8,128)})) conditional(s32[]{:T(128)} %convert_element_type.229, (f32[2,256]{1,0:T(2,128)S(1)}, f32[2,256]{1,0:T(2,128)S(1)}, f32[256,2,128]{0,2,1:T(8,128)}) %tuple.58, (s32[]{:T(128)}, s32[]{:T(128)}, bf16[2048,256]{1,0:T(8,128)(2,1)}, ...), branch_computations={%region_2.0_spmd, %region_3.5_spmd} | conditional | flops 610142976 | bytes 22129834 | solution.py:135
  54.9 1.5 convolution_convert_fusion.1
  56.4 0.5 fusion.81
  56.9 0.2 broadcast_compare_fusion
  57.1 0.6 fusion.80
  57.7 0.6 copy-done.1
  58.3 0.3 convolution_convert_fusion
  58.7 0.6 fusion.6
  59.3 0.4 fusion.5
  59.7 0.3 copy-done.7
  60.1 1.0 divide_convert_fusion
  61.1 1.5 convolution_convert_fusion.3
  62.7 0.1 eq.29
  62.8 0.1 eq.25
  62.9 0.6 reduce-window.6
  63.5 0.2 slice_reduce_fusion
  63.8 0.1 copy.28
  63.9 0.1 mul.231
  64.1 1.4 scatter_custom_fusion
  65.5 25.8 %reduce-scatter.2.cloned.1.call-done = bf16[64,2048]{1,0:T(8,128)(2,1)} async-done(((bf16[256,2048]{1,0:T(8,128)(2,1)}), bf16[64,2048]{1,0:T(8,128)(2,1)}) %reduce-scatter.2.cloned.1.call-update) | async-done | bytes 262160 | tf_op jit(solution)/shard_map/reduce_scatter | solution.py:144
  91.3 1.1 fusion.51
  92.5 1.1 fusion.53
  93.6 3.3 %gather_fusion = bf16[512,2048]{1,0:T(8,128)(2,1)} fusion(bf16[65,2048]{1,0:T(8,128)(2,1)S(1)} %concatenate.22, s32[1024]{0:T(1024)S(1)} %pad_clamp_fusion.1), kind=kCustom, calls=%fused_computation | custom fusion | bytes 4196352 | tf_op jit(solution)/shard_map/gather | solution.py:167
  97.0 53.7 %all_to_all.10 = bf16[8,64,2048]{2,1,0:T(8,128)(2,1)S(1)} all-to-all(bf16[8,64,2048]{2,1,0:T(8,128)(2,1)} %bitcast.107), channel_id=1, replica_groups=mesh['sp'=8,'tp'=4] {'sp'}, dimensions={0} | all-to-all | bytes 4194304 | tf_op jit(solution)/shard_map/all_to_all | solution.py:168
  150.7 1.3 copy-done.4
  152.0 1.2 fusion.28
  153.2 5.8 %convolution_convert_fusion.2 = bf16[8,64,2048]{2,1,0:T(8,128)(2,1)} fusion(bf16[1,384,2048]{2,1,0:T(8,128)(2,1)S(1)} %copy-done, bf16[8,64,2048]{2,1,0:T(8,128)(2,1)} %copy-done.4, bf16[1,2048,384]{2,1,0:T(8,128)(2,1)} %param.35, f32[8,1,64,384]{3,2,0,1:T(8,128)S(1)} %fusion.28), kind=kOutput, calls=%fused_computation.31 | convolution fusion | flops 1612840960 | bytes 8126464 | tf_op jit(solution)/shard_map/seif,efd->seid/dot_general | solution.py:178
  159.0 4.7 %all-to-all-start.1 = ((bf16[8,64,2048]{2,1,0:T(8,128)(2,1)}), bf16[8,64,2048]{2,1,0:T(8,128)(2,1)}, u32[]{:S(2)}, u32[]{:S(2)}) async-start(bf16[8,64,2048]{2,1,0:T(8,128)(2,1)} %convolution_convert_fusion.2), calls=%async_computation.2 | async-start | bytes 4194304 | tf_op jit(solution)/shard_map/all_to_all | solution.py:182
  163.8 1.8 fusion.82
  165.6 45.3 %all-to-all-done.1 = bf16[8,64,2048]{2,1,0:T(8,128)(2,1)} async-done(((bf16[8,64,2048]{2,1,0:T(8,128)(2,1)}), bf16[8,64,2048]{2,1,0:T(8,128)(2,1)}, u32[]{:S(2)}, u32[]{:S(2)}) %all-to-all-start.1) | async-done | bytes 2097184 | tf_op jit(solution)/shard_map/all_to_all | solution.py:182
  210.8 4.2 %gather_fusion.1 = bf16[256,2048]{1,0:T(8,128)(2,1)S(1)} fusion(bf16[512,2048]{1,0:T(8,128)(2,1)} %bitcast.35, s32[1024]{0:T(1024)S(1)} %pad_clamp_fusion), kind=kCustom, calls=%fused_computation.1 | custom fusion | bytes 2098176 | tf_op jit(solution)/shard_map/gather | solution.py:183
  215.1 1.7 reshape.303
  216.8 3.2 %multiply_reduce_fusion = bf16[64,2048]{1,0:T(8,128)(2,1)S(1)} fusion(f32[64,4,2048]{2,1,0:T(4,128)} %reshape.303, f32[64,4]{1,0:T(8,128)S(1)} %copy.31), kind=kLoop, calls=%fused_computation.37 | loop fusion | flops 917504 | bytes 2360320 | tf_op jit(solution)/shard_map/reduce_sum | solution.py:184
  220.0 3.4 %fusion.22 = bf16[64,2048]{1,0:T(8,128)(2,1)} fusion(bf16[384,2048]{1,0:T(8,128)(2,1)} %param.39, bf16[64,2048]{1,0:T(8,128)(2,1)S(1)} %fusion.53, bf16[2048,384]{1,0:T(8,128)(2,1)} %param.38, bf16[64,2048]{1,0:T(8,128)(2,1)S(1)} %multiply_reduce_fusion, f32[64,384]{1,0:T(8,128)S(1)} %fusion.82, bf16[64,2048]{1,0:T(8,128)(2,1)S(1)} %copy-done.3, ...), kind=kOutput, calls=%fused_computation.36 | convolution fusion | flops 202915840 | bytes 4554752 | tf_op jit(solution)/shard_map/dot_general | solution.py:193
  (57 shorter events, 0.6 us)
Async XLA Ops:
  6.5 146.7 %copy-start = (bf16[1,384,2048]{2,1,0:T(8,128)(2,1)S(1)}, bf16[1,384,2048]{2,1,0:T(8,128)(2,1)}, u32[]{:S(2)}) copy-start(bf16[1,384,2048]{2,1,0:T(8,128)(2,1)} %param.36) | copy-start | bytes 4718596
  6.5 47.6 %all-gather.2.cloned.1.call-start = ((), (), s32[]{:S(2)}) async-start(), calls=%async_computation.3 | async-start | bytes 1179648 | tf_op jit(solution)/shard_map/all_gather | solution.py:118
  10.0 81.3 %reduce-scatter.2.cloned.1.call-start = ((), (), s32[]{:S(2)}) async-start(), calls=%async_computation.4 | async-start | bytes 1310720 | tf_op jit(solution)/shard_map/reduce_scatter | solution.py:144
  54.8 6.3 %copy-start.5 = (bf16[256,2048]{1,0:T(8,128)(2,1)S(1)}, bf16[256,2048]{1,0:T(8,128)(2,1)}, u32[]{:S(2)}) copy-start(bf16[256,2048]{1,0:T(8,128)(2,1)} %param.29) | copy-start | bytes 3145732
  57.1 1.2 copy-start.1
  57.1 1.6 copy-start.6
  59.3 0.7 copy-start.7
  60.0 2.5 %copy-start.8 = (s32[64,4]{0,1:T(4,128)S(1)}, s32[64,4]{0,1:T(4,128)}, u32[]{:S(2)}) copy-start(s32[64,4]{0,1:T(4,128)} %param.32) | copy-start | bytes 3076
  60.1 2.9 %copy-start.9 = (bf16[2048]{0:T(1024)(128)(2,1)S(1)}, bf16[2048]{0:T(1024)(128)(2,1)}, u32[]{:S(2)}) copy-start(bf16[2048]{0:T(1024)(128)(2,1)} %param.31) | copy-start | bytes 12292
  60.1 31.3 %copy-start.2 = (bf16[64,2048]{1,0:T(8,128)(2,1)S(1)}, bf16[64,2048]{1,0:T(8,128)(2,1)}, u32[]{:S(2)}) copy-start(bf16[64,2048]{1,0:T(8,128)(2,1)} %param.30) | copy-start | bytes 786436
  97.0 55.0 %copy-start.11 = (bf16[1,2048,384]{2,1,0:T(8,128)(2,1)S(1)}, bf16[1,2048,384]{2,1,0:T(8,128)(2,1)}, u32[]{:S(2)}) copy-start(bf16[1,2048,384]{2,1,0:T(8,128)(2,1)} %param.34) | copy-start | bytes 4718596
  150.7 1.3 copy-start.4
  159.0 4.7 %copy-start.10 = (f32[64,4]{0,1:T(4,128)S(1)}, f32[64,4]{0,1:T(4,128)}, u32[]{:S(2)}) copy-start(f32[64,4]{0,1:T(4,128)} %param.33) | copy-start | bytes 3076
  159.0 51.8 %all-to-all-start.1 = ((bf16[8,64,2048]{2,1,0:T(8,128)(2,1)}), bf16[8,64,2048]{2,1,0:T(8,128)(2,1)}, u32[]{:S(2)}, u32[]{:S(2)}) async-start(bf16[8,64,2048]{2,1,0:T(8,128)(2,1)} %convolution_convert_fusion.2), calls=%async_computation.2 | async-start | bytes 4194304 | tf_op jit(solution)/shard_map/all_to_all | solution.py:182
  215.1 4.9 %copy-start.3 = (bf16[64,2048]{1,0:T(8,128)(2,1)S(1)}, bf16[64,2048]{1,0:T(8,128)(2,1)}, u32[]{:S(2)}) copy-start(bf16[64,2048]{1,0:T(8,128)(2,1)} %reduce-scatter.2.cloned.1.call-done) | copy-start | bytes 786436
Sparse Core Ops, SparseCore 0:
  10.2 43.9 all-gather.1
  62.7 28.5 reduce-scatter.1
where the time goes:
time: 231 us; the launch traced here: 230 us
  blocking collectives  86.8 us (38%)
  waiting for transfers between devices  77.7 us (34%)
  local copies, waits for them, and re-layouts  17.5 us (8%)
  matrix products  17.1 us (7%)
  between operations  13.7 us (6%)
  other arithmetic  12.5 us (5%)
  starting transfers between devices  4.73 us (2%)
    all_to_all x1, blocking collectives, body(): lax.all_to_all(outgoing, 'sp', split_axis=0, concat_axis=0, tiled=True)  53.7 us
    all_to_all x1, waiting for transfers between devices, body(): lax.all_to_all(answered, 'sp', split_axis=0, concat_axis=0, tiled=True)  45.3 us
    all_gather x1, blocking collectives, body(): lax.all_gather(rot_key, 'sp', axis=0, tiled=True)  33.1 us
    reduce_scatter x1, waiting for transfers between devices, body(): lax.psum_scatter(jnp.dot(heads_out, out_proj, preferred_element_type=jnp....  25.8 us
    all_gather x1, waiting for transfers between devices, body(): lax.all_gather(normed_latent, 'sp', axis=0, tiled=True)  6.64 us
    dot_general x1, matrix products, body(): jnp.einsum('seif,efd->seid', expert_hidden, expert_down, preferred_elemen...  5.77 us
    all_to_all x1, starting transfers between devices, body(): lax.all_to_all(answered, 'sp', split_axis=0, concat_axis=0, tiled=True)  4.68 us
  transfers between devices with their start and end apart: 3, of which 3 were waited for; matrix products, arithmetic and copies ran while one was open for 4% of the time, Pallas kernels for 0%

commit v1 on v0

--- a/solution.py
+++ b/solution.py
@@ -1,8 +1,11 @@
+import functools
 import math
 
 import jax
 import jax.numpy as jnp
 from jax import lax
+from jax.experimental import pallas as pl
+from jax.experimental.pallas import tpu as pltpu
 from jax.sharding import PartitionSpec as P
 
 NOPE = 128
@@ -38,7 +41,7 @@
     ).astype(jnp.bfloat16)
 
 
-def body(
+def start_body(
     query_nope,
     query_rope,
     latent,
@@ -200,6 +203,473 @@
     ).astype(jnp.bfloat16)
 
 
+MESH = pl.DeviceIdType.MESH
+F32 = jnp.float32
+BF16 = jnp.bfloat16
+LANES = 128
+
+
+def arrived(ref, sem):
+    pltpu.make_async_copy(ref, ref, sem).wait()
+
+
+def greet(z, depth, me, tp_peers):
+    barrier = pltpu.get_barrier_semaphore()
+
+    @pl.when(z + 1 < depth)
+    def _():
+        pl.semaphore_signal(barrier, inc=1, device_id={"sp": me + 2}, device_id_type=MESH)
+
+    @pl.when(z > 0)
+    def _():
+        pl.semaphore_signal(barrier, inc=1, device_id={"sp": me - 2}, device_id_type=MESH)
+
+    pair = z * 4 + 1 - me
+    pl.semaphore_signal(barrier, inc=1, device_id={"sp": pair}, device_id_type=MESH)
+    for peer in tp_peers:
+        pl.semaphore_signal(barrier, inc=1, device_id={"tp": peer}, device_id_type=MESH)
+    line_peers = (z + 1 < depth).astype(jnp.int32) + (z > 0).astype(jnp.int32)
+    pl.semaphore_wait(barrier, 1 + len(tp_peers) + line_peers)
+
+
+class Gather:
+    def __init__(self, view, up, down, side, got, z, x, depth, relay=None):
+        self.view, self.up, self.down, self.side, self.got = view, up, down, side, got
+        self.z, self.x, self.depth, self.relay = z, x, depth, relay
+        self.me = z * 2 + x
+
+    def copy(self, block, sem, to):
+        return pltpu.make_async_remote_copy(
+            src_ref=self.view(block), dst_ref=self.view(block), send_sem=sem,
+            recv_sem=self.got.at[block], device_id={"sp": to}, device_id_type=MESH)
+
+    def send_up(self, zz):
+        return self.copy(zz * 2 + self.x, self.up.at[zz], self.me + 2)
+
+    def send_down(self, zz):
+        return self.copy(zz * 2 + self.x, self.down.at[zz], self.me - 2)
+
+    def send_side(self, zz):
+        return self.copy(zz * 2 + self.x, self.side.at[zz], self.z * 2 + 1 - self.x)
+
+    def start(self):
+        z = self.z
+
+        @pl.when(z + 1 < self.depth)
+        def _():
+            self.send_up(z).start()
+
+        @pl.when(z > 0)
+        def _():
+            self.send_down(z).start()
+
+        self.send_side(z).start()
+
+    def run(self):
+        z, x, depth = self.z, self.x, self.depth
+        for j in range(1, depth):
+            @pl.when(z - j >= 0)
+            def _():
+                zz = z - j
+                arrived(self.view(zz * 2 + x), self.got.at[zz * 2 + x])
+
+                @pl.when(z + 1 < depth)
+                def _():
+                    self.send_up(zz).start()
+
+                self.send_side(zz).start()
+                if self.relay is not None:
+                    self.relay(zz * 2 + x)
+
+            @pl.when(z + j < depth)
+            def _():
+                zz = z + j
+                arrived(self.view(zz * 2 + x), self.got.at[zz * 2 + x])
+
+                @pl.when(z > 0)
+                def _():
+                    self.send_down(zz).start()
+
+                self.send_side(zz).start()
+                if self.relay is not None:
+                    self.relay(zz * 2 + x)
+
+        def crossed(zz):
+            block = zz * 2 + 1 - x
+            arrived(self.view(block), self.got.at[block])
+            if self.relay is not None:
+                self.relay(block)
+
+        crossed(z)
+        for j in range(1, depth):
+            @pl.when(z - j >= 0)
+            def _():
+                crossed(z - j)
+
+            @pl.when(z + j < depth)
+            def _():
+                crossed(z + j)
+
+    def finish(self):
+        z, depth = self.z, self.depth
+        for zz in range(depth):
+            @pl.when((zz <= z) & (z + 1 < depth))
+            def _():
+                self.send_up(zz).wait_send()
+
+            @pl.when((zz >= z) & (z > 0))
+            def _():
+                self.send_down(zz).wait_send()
+
+            self.send_side(zz).wait_send()
+
+
+def latent_kernel(depth, own_ref, out_ref, up, down, side, got, relay_out, relay_in):
+    me = lax.axis_index("sp")
+    t = lax.axis_index("tp")
+    z, x = me // 2, me % 2
+    half = t % 2
+    sibling = t + 1 - 2 * half
+    greet(z, depth, me, [sibling])
+    out_ref[me] = own_ref[...]
+
+    def relay_copy(block):
+        return pltpu.make_async_remote_copy(
+            src_ref=out_ref.at[block, half], dst_ref=out_ref.at[block, half],
+            send_sem=relay_out.at[block], recv_sem=relay_in.at[block],
+            device_id={"tp": sibling}, device_id_type=MESH)
+
+    ring = Gather(lambda b: out_ref.at[b, half], up, down, side, got, z, x, depth,
+                  relay=lambda b: relay_copy(b).start())
+    ring.start()
+    ring.run()
+    for block in range(2 * depth):
+        @pl.when(block != me)
+        def _():
+            arrived(out_ref.at[block, 1 - half], relay_in.at[block])
+            relay_copy(block).wait_send()
+    ring.finish()
+
+
+def gather_latents(packed, sp):
+    depth = sp // 2
+    rows, width = packed.shape
+    dma = pltpu.SemaphoreType.DMA
+    out = pl.pallas_call(
+        functools.partial(latent_kernel, depth),
+        out_shape=jax.ShapeDtypeStruct((sp, 2, rows // 2, width), packed.dtype),
+        in_specs=[pl.BlockSpec(memory_space=pltpu.VMEM)],
+        out_specs=pl.BlockSpec(memory_space=pltpu.VMEM),
+        scratch_shapes=[dma((depth,)), dma((depth,)), dma((depth,)), dma((sp,)), dma((sp,)), dma((sp,))],
+        compiler_params=pltpu.CompilerParams(collective_id=0, has_side_effects=True),
+        name="latent_gather",
+    )(packed.reshape(2, rows // 2, width))
+    return out.reshape(sp, rows, width)
+
+
+def gated(rows, gate, up, down):
+    gate_part = jnp.dot(rows, gate[...], preferred_element_type=F32)
+    upper = jnp.dot(rows, up[...], preferred_element_type=F32)
+    hidden = (gate_part / (1.0 + jnp.exp(-gate_part)) * upper).astype(BF16)
+    return jnp.dot(hidden, down[...], preferred_element_type=F32).astype(BF16)
+
+
+def tail_kernel(depth, chips, experts,
+                heads_ref, proj_ref, resid_ref, gain_ref, route_ref,
+                eg_hbm, eu_hbm, ed_hbm, sg_hbm, su_hbm, sd_hbm,
+                out_ref,
+                eg, eu, ed, sg, su, sd, load_sem,
+                part, sib, ysend, yrecv, sib_s, sib_r, y_s, y_r,
+                hid, shared, xbuf, up, down, side, got,
+                contrib, xr, upr, dnr, rx_s, rx_r, rz_s, up_r, dn_r):
+    me = lax.axis_index("sp")
+    t = lax.axis_index("tp")
+    z, x = me // 2, me % 2
+    y, c = t // 2, t % 2
+    tokens, width = resid_ref.shape
+    loads = [pltpu.make_async_copy(src, dst, load_sem.at[i]) for i, (src, dst) in enumerate(
+        ((sg_hbm, sg), (su_hbm, su), (sd_hbm, sd), (eg_hbm.at[0], eg), (eu_hbm.at[0], eu), (ed_hbm.at[0], ed)))]
+    for load in loads:
+        load.start()
+    sibling = t + 1 - 2 * c
+    peers = [lax.rem(t + 2 * d, 2 * chips) for d in range(1, chips)]
+    greet(z, depth, me, [sibling] + peers)
+
+    def project(block):
+        rows = heads_ref[pl.ds(pl.multiple_of(block * tokens, tokens), tokens), :]
+        return jnp.dot(rows, proj_ref[...], preferred_element_type=F32).astype(BF16)
+
+    def to_sibling(yy):
+        return pltpu.make_async_remote_copy(
+            src_ref=part.at[yy], dst_ref=sib.at[yy], send_sem=sib_s.at[yy], recv_sem=sib_r.at[yy],
+            device_id={"tp": sibling}, device_id_type=MESH)
+
+    def to_chip(d):
+        return pltpu.make_async_remote_copy(
+            src_ref=ysend.at[d - 1], dst_ref=yrecv.at[d - 1], send_sem=y_s.at[d - 1], recv_sem=y_r.at[d - 1],
+            device_id={"tp": peers[d - 1]}, device_id_type=MESH)
+
+    ahead = [lax.rem(y + d, chips) for d in range(1, chips)] + [y]
+    for yy in ahead:
+        part[yy] = project(yy * 2 + 1 - c)
+        to_sibling(yy).start()
+    for d in range(1, chips):
+        yy = ahead[d - 1]
+        mine = project(yy * 2 + c).astype(F32)
+        arrived(sib.at[yy], sib_r.at[yy])
+        ysend[d - 1] = (mine + sib[yy].astype(F32)).astype(BF16)
+        to_chip(d).start()
+    total = project(y * 2 + c).astype(F32)
+    arrived(sib.at[y], sib_r.at[y])
+    total = total + sib[y].astype(F32)
+    for d in range(1, chips):
+        arrived(yrecv.at[d - 1], y_r.at[d - 1])
+        total = total + yrecv[d - 1].astype(F32)
+    hidden_one = (resid_ref[...].astype(F32) + total).astype(BF16)
+    hid[...] = hidden_one
+    wide = hidden_one.astype(F32)
+    factor = lax.rsqrt(jnp.mean(wide * wide, axis=-1, keepdims=True) + norm_eps)
+    xbuf[me, :, :width] = (wide * factor * gain_ref[...].astype(F32)).astype(BF16)
+    xbuf[me, :, width:] = route_ref[...]
+
+    ring = Gather(lambda b: xbuf.at[b], up, down, side, got, z, x, depth)
+    ring.start()
+    for load in loads[:3]:
+        load.wait()
+    shared[...] = gated(xbuf[me, :, :width], sg, su, sd)
+    ring.run()
+    for load in loads[3:]:
+        load.wait()
+
+    def cross(zz):
+        return pltpu.make_async_remote_copy(
+            src_ref=contrib.at[zz, 1 - x], dst_ref=xr.at[zz], send_sem=rx_s.at[zz], recv_sem=rx_r.at[zz],
+            device_id={"sp": z * 2 + 1 - x}, device_id_type=MESH)
+
+    high = (z >= depth // 2).astype(jnp.int32)
+
+    def expert_step(j, carry):
+        pick = high * j + (1 - high) * (depth - 2 - j)
+        pick = pick + (pick >= z).astype(jnp.int32)
+        last = (j == depth - 1).astype(jnp.int32)
+        zz = last * z + (1 - last) * pick
+        pair = xbuf[pl.ds(zz * 2, 2)].reshape(2 * tokens, width + LANES)
+        routes = pair[:, width:].astype(F32)
+        lane = lax.broadcasted_iota(jnp.int32, routes.shape, 1)
+        weight = jnp.sum(jnp.where((lane == me) | (lane == me + experts), routes, 0.0), axis=1, keepdims=True)
+        rows = gated(pair[:, :width], eg, eu, ed).astype(F32) * weight
+        contrib[zz] = rows.astype(BF16).reshape(2, tokens, width)
+        cross(zz).start()
+        return carry
+
+    lax.fori_loop(0, depth, expert_step, 0)
+
+    def pass_up(dst):
+        return pltpu.make_async_remote_copy(
+            src_ref=contrib.at[dst, x], dst_ref=upr.at[dst], send_sem=rz_s.at[dst], recv_sem=up_r.at[dst],
+            device_id={"sp": me + 2}, device_id_type=MESH)
+
+    def pass_down(dst):
+        return pltpu.make_async_remote_copy(
+            src_ref=contrib.at[dst, x], dst_ref=dnr.at[dst], send_sem=rz_s.at[dst], recv_sem=dn_r.at[dst],
+            device_id={"sp": me - 2}, device_id_type=MESH)
+
+    def local_sum(dst):
+        arrived(xr.at[dst], rx_r.at[dst])
+        return contrib[dst, x].astype(F32) + xr[dst].astype(F32)
+
+    for k in range(depth - 1):
+        @pl.when(depth - 1 - k > z)
+        def _():
+            dst = depth - 1 - k
+
+            @pl.when(z > 0)
+            def _():
+                arrived(upr.at[dst], up_r.at[dst])
+                contrib[dst, x] = (local_sum(dst) + upr[dst].astype(F32)).astype(BF16)
+
+            @pl.when(z == 0)
+            def _():
+                contrib[dst, x] = local_sum(dst).astype(BF16)
+
+            pass_up(dst).start()
+
+        @pl.when(k < z)
+        def _():
+            dst = k
+
+            @pl.when(z + 1 < depth)
+            def _():
+                arrived(dnr.at[dst], dn_r.at[dst])
+                contrib[dst, x] = (local_sum(dst) + dnr[dst].astype(F32)).astype(BF16)
+
+            @pl.when(z + 1 == depth)
+            def _():
+                contrib[dst, x] = local_sum(dst).astype(BF16)
+
+            pass_down(dst).start()
+
+    @pl.when(z == 0)
+    def _():
+        upr[z] = jnp.zeros(upr.shape[1:], BF16)
+
+    @pl.when(z > 0)
+    def _():
+        arrived(upr.at[z], up_r.at[z])
+
+    @pl.when(z + 1 == depth)
+    def _():
+        dnr[z] = jnp.zeros(dnr.shape[1:], BF16)
+
+    @pl.when(z + 1 < depth)
+    def _():
+        arrived(dnr.at[z], dn_r.at[z])
+
+    routed = (local_sum(z) + upr[z].astype(F32) + dnr[z].astype(F32)).astype(BF16)
+    out_ref[...] = (hid[...].astype(F32) + routed.astype(F32) + shared[...].astype(F32)).astype(BF16)
+
+    for yy in range(chips):
+        to_sibling(yy).wait_send()
+    for d in range(1, chips):
+        to_chip(d).wait_send()
+    ring.finish()
+    for zz in range(depth):
+        cross(zz).wait_send()
+
+        @pl.when(zz != z)
+        def _():
+            pltpu.make_async_copy(contrib.at[zz, x], contrib.at[zz, x], rz_s.at[zz]).wait()
+
+
+def finish_layer(sp, tp, heads_out, out_proj, residual, ffn_gain, routes, eg, eu, ed, sg, su, sd):
+    depth, chips = sp // 2, tp // 2
+    tokens, width = residual.shape
+    ff = sg.shape[1]
+    dma = pltpu.SemaphoreType.DMA
+    vmem = pl.BlockSpec(memory_space=pltpu.VMEM)
+    hbm = pl.BlockSpec(memory_space=pl.ANY)
+    block = (tokens, width)
+    experts = sp
+
+    def buf(*shape):
+        return pltpu.VMEM(shape, BF16)
+
+    scratch = [
+        buf(width, ff), buf(width, ff), buf(ff, width), buf(width, ff), buf(width, ff), buf(ff, width), dma((6,)),
+        buf(chips, *block), buf(chips, *block), buf(chips - 1, *block), buf(chips - 1, *block),
+        dma((chips,)), dma((chips,)), dma((chips - 1,)), dma((chips - 1,)),
+        buf(*block), buf(*block), buf(sp, tokens, width + LANES),
+        dma((depth,)), dma((depth,)), dma((depth,)), dma((sp,)),
+        buf(depth, 2, *block), buf(depth, *block), buf(depth, *block), buf(depth, *block),
+        dma((depth,)), dma((depth,)), dma((depth,)), dma((depth,)), dma((depth,)),
+    ]
+    return pl.pallas_call(
+        functools.partial(tail_kernel, depth, chips, experts),
+        out_shape=jax.ShapeDtypeStruct(block, BF16),
+        in_specs=[vmem] * 5 + [hbm] * 6,
+        out_specs=vmem,
+        scratch_shapes=scratch,
+        compiler_params=pltpu.CompilerParams(
+            collective_id=1, has_side_effects=True, vmem_limit_bytes=48 * 1024 * 1024),
+        name="layer_tail",
+    )(heads_out, out_proj, residual, ffn_gain.reshape(1, -1), routes, eg, eu, ed, sg, su, sd)
+
+
+def attention(row_count, local_heads, queries_nope, rot_query, key_local, value_local, positions, last_row, pieces):
+    score_scale = 1.0 / math.sqrt(NOPE + ROPE)
+
+    def expand(block_latent):
+        keys_flat = jnp.dot(block_latent, key_local, preferred_element_type=jnp.float32).astype(BF16)
+        values_flat = jnp.dot(block_latent, value_local, preferred_element_type=jnp.float32).astype(BF16)
+        return (keys_flat, values_flat)
+
+    def attend(state_now, keys_flat, values_flat, keys_rope, key_start):
+        running, weight_sum, weighted = state_now
+        key_count = keys_flat.shape[0]
+        key_heads = keys_flat.reshape(key_count, local_heads, NOPE)
+        value_heads = values_flat.reshape(key_count, local_heads, VDIM)
+        scores = jnp.einsum("qhd,khd->hqk", queries_nope, key_heads, preferred_element_type=jnp.float32)
+        scores = (
+            scores + jnp.einsum("qhd,kd->hqk", rot_query, keys_rope, preferred_element_type=jnp.float32)
+        ) * score_scale
+        key_pos = key_start + jnp.arange(key_count, dtype=jnp.int32)
+        allowed = (key_pos[None, :] <= positions[:, None])[None]
+        scores = jnp.where(allowed, scores, -1e30)
+        newest = jnp.maximum(running, jnp.max(scores, axis=-1))
+        weights = jnp.where(allowed, jnp.exp(scores - newest[..., None]), 0.0)
+        shrink = jnp.exp(running - newest)
+        weight_sum = weight_sum * shrink + jnp.sum(weights, axis=-1)
+        mixed = jnp.einsum("hqk,khd->qhd", weights.astype(BF16), value_heads, preferred_element_type=jnp.float32)
+        weighted = weighted * shrink.T[:, :, None] + mixed
+        return (newest, weight_sum, weighted)
+
+    initial = (
+        jnp.full((local_heads, row_count), -jnp.inf, jnp.float32),
+        jnp.zeros((local_heads, row_count), jnp.float32),
+        jnp.zeros((row_count, local_heads, VDIM), jnp.float32),
+    )
+    piece_len = pieces[0].shape[0]
+    span_len = math.gcd(piece_len, 1024)
+
+    def advance(step_num, state_in):
+        offset = step_num * span_len
+        sliced = tuple((lax.dynamic_slice_in_dim(member, offset, span_len, 0) for member in pieces))
+
+        def compute(state_cur):
+            keys_flat, values_flat = expand(sliced[0])
+            return attend(state_cur, keys_flat, values_flat, sliced[-1], offset)
+
+        return lax.cond(offset <= last_row, compute, lambda state_cur: state_cur, state_in)
+
+    folded = lax.fori_loop(0, piece_len // span_len, advance, initial)
+    return (folded[2] / folded[1].T[:, :, None]).astype(BF16).reshape(row_count, local_heads * VDIM)
+
+
+def line_body(query_nope, query_rope, latent, key_rope, latent_gain, key_up, value_up, out_proj, residual, ffn_gain,
+              expert_ids, route_weights, expert_gate, expert_up, expert_down, shared_gate, shared_up, shared_down):
+    sp, tp = lax.axis_size("sp"), lax.axis_size("tp")
+    row_count, rank = latent.shape
+    first_row = lax.axis_index("sp") * row_count
+    last_row = first_row + row_count - 1
+    positions = first_row + jnp.arange(row_count, dtype=jnp.int32)
+    local_heads = query_nope.shape[1] // NOPE
+    head_start = lax.axis_index("tp") * local_heads
+    normed_latent = scale_rows(latent, latent_gain)
+    rot_key = rotate(key_rope[:, None, :], positions)[:, 0, :]
+    rope_rows = row_count * ROPE // rank
+    packed = jnp.concatenate([normed_latent, rot_key.reshape(rope_rows, rank)], axis=0)
+    gathered = gather_latents(packed, sp)
+    pieces = (
+        gathered[:, :row_count].reshape(sp * row_count, rank),
+        gathered[:, row_count:].reshape(sp * row_count, ROPE),
+    )
+    key_local = lax.dynamic_slice_in_dim(key_up, head_start * NOPE, local_heads * NOPE, 1)
+    value_local = lax.dynamic_slice_in_dim(value_up, head_start * VDIM, local_heads * VDIM, 1)
+    queries_nope = query_nope.reshape(row_count, local_heads, NOPE)
+    rot_query = rotate(query_rope.reshape(row_count, local_heads, ROPE), positions)
+    heads_out = attention(
+        row_count, local_heads, queries_nope, rot_query, key_local, value_local, positions, last_row, pieces)
+    chosen = expert_ids[:, :, None] == jnp.arange(sp, dtype=jnp.int32)
+    dense = jnp.sum(jnp.where(chosen, route_weights[:, :, None], 0.0), axis=1)
+    coarse = lax.reduce_precision(dense, 8, 7)
+    fine = dense - coarse
+    routes = jnp.pad(jnp.concatenate([coarse, fine], axis=1), ((0, 0), (0, LANES - 2 * sp))).astype(BF16)
+    return finish_layer(sp, tp, heads_out, out_proj, residual, ffn_gain, routes,
+                        expert_gate, expert_up, expert_down, shared_gate, shared_up, shared_down)
+
+
+def body(*args):
+    latent, residual, expert_ids, expert_gate = args[2], args[8], args[10], args[12]
+    sp, tp = lax.axis_size("sp"), lax.axis_size("tp")
+    tokens, slots = residual.shape[0], expert_ids.shape[1]
+    experts = expert_gate.shape[0] * sp
+    capacity = 2 * tokens * slots // experts
+    dense = capacity >= tokens and expert_gate.shape[0] == 1
+    if dense and sp % 2 == 0 and tp % 2 == 0 and tp > 2 and 2 * sp <= LANES:
+        return line_body(*args)
+    return start_body(*args)
+
+
 def solution(mesh):
     in_specs = (
         P("sp", "tp"),

time: 231 us -> 128 us (0.55)
  Pallas kernels: 0 us -> 99.7 us
  blocking collectives: 86.8 us -> 0 us
  waiting for transfers between devices: 77.7 us -> 0 us
  between operations: 13.7 us -> 0.18 us
  matrix products: 17.1 us -> 4.42 us
  starting transfers between devices: 4.73 us -> 0 us
  other arithmetic: 12.5 us -> 8.79 us
  local copies, waits for them, and re-layouts: 17.5 us -> 14.1 us
    pallas_call x0 -> x2, Pallas kernels: none -> 99.7 us  [the longest x1 78.3 us: finish_layer(): pl.pallas_call(functools.partial(tail_kernel, depth, chips, experts), out...]
    all_to_all x1 -> x0, blocking collectives: 53.7 us -> none  [body(): lax.all_to_all(outgoing, 'sp', split_axis=0, concat_axis=0, tiled=True)]
    all_to_all x1 -> x0, waiting for transfers between devices: 45.3 us -> none  [body(): lax.all_to_all(answered, 'sp', split_axis=0, concat_axis=0, tiled=True)]
    all_gather x1 -> x0, blocking collectives: 33.1 us -> none  [body(): lax.all_gather(rot_key, 'sp', axis=0, tiled=True)]
    reduce_scatter x1 -> x0, waiting for transfers between devices: 25.8 us -> none  [body(): lax.psum_scatter(jnp.dot(heads_out, out_proj, preferred_element_type=jnp....]
    dot_general x6 -> x1, matrix products: 14.2 us -> 0.57 us  [attend(): jnp.einsum('hqk,khd->qhd', weights.astype(BF16), value_heads, preferred_e...]
    gather x2 -> x0, local copies, waits for them, and re-layouts: 7.57 us -> none  [the longest x1 4.22 us: body(): picked = returned.reshape(experts * capacity, model_width)[target]]
    all_gather x1 -> x0, waiting for transfers between devices: 6.64 us -> none  [body(): lax.all_gather(normed_latent, 'sp', axis=0, tiled=True)]
  transfers between devices with their start and end apart: 3 -> 0, of which waited for: 3 -> 0; matrix products, arithmetic and copies ran while one was open for 4% -> 0% of each run, Pallas kernels for 0% -> 0%
where the time goes in v1:
time: 128 us; the launch traced here: 127 us
  Pallas kernels  99.7 us (78%)
  local copies, waits for them, and re-layouts  14.1 us (11%)
  other arithmetic  8.79 us (7%)
  matrix products  4.42 us (3%)
    pallas_call x1, Pallas kernels, finish_layer(): pl.pallas_call(functools.partial(tail_kernel, depth, chips, experts), out...  78.3 us
    pallas_call x1, Pallas kernels, gather_latents(): pl.pallas_call(functools.partial(latent_kernel, depth), out_shape=jax.Sha...  21.3 us
    unnamed x16, local copies, waits for them, and re-layouts  3.71 us

profile of v1, /device:TPU:0, one launch (start us, length us, event | category | flops | bytes accessed | tf_op | source)
XLA Modules:
  0.0 127.5 jit_solution(3783621521098815926)
XLA Ops:
  0.0 0.2 multiply_cosine_fusion
  0.2 0.9 copy.50
  1.2 0.6 pad_maximum_fusion.1
  1.8 0.8 bitcast_convert_fusion
  2.6 0.2 fusion.28
  2.8 0.1 copy.48
  2.9 0.1 convert_element_type.74
  3.1 1.0 fusion.20
  4.1 0.7 convert_element_type.69
  4.7 1.0 fusion.22
  5.8 0.7 pad_maximum_fusion
  6.4 21.3 %latent_gather.1 = bf16[8,2,160,256]{3,2,1,0:T(8,128)(2,1)} custom-call(bf16[2,160,256]{2,1,0:T(8,128)(2,1)} %bitcast.44), custom_call_target="tpu_custom_call" | custom-call | tf_op jit(solution)/shard_map/latent_gather/pallas_call | solution.py:358
  27.8 0.0 copy-start.9
  27.8 2.3 %slice.26 = bf16[8,256,256]{2,1,0:T(8,128)(2,1)} slice(bf16[8,320,256]{2,1,0:T(8,128)(2,1)} %bitcast.42), slice={[0:8], [0:256], [0:256]} | slice | bytes 2097152 | tf_op jit(solution)/shard_map/slice | solution.py:643
  30.1 1.0 slice.27
  31.1 0.2 reshape.211
  31.3 0.9 copy.52
  32.2 1.6 %constant_dynamic-slice_fusion = (bf16[256,256]{1,0:T(8,128)(2,1)S(1)}, bf16[256,256]{1,0:T(8,128)(2,1)}) fusion(bf16[256,1024]{1,0:T(8,128)(2,1)} %param.28, s32[]{:T(128)S(6)} %select_n.31, bf16[256,1024]{1,0:T(8,128)(2,1)} %param.27), kind=kLoop, calls=%fused_computation.61 | loop fusion | bytes 524292 | tf_op jit(solution)/shard_map/dynamic_slice | solution.py:647
  33.9 0.1 copy.49
  34.0 0.8 copy.51
  34.7 0.7 broadcast_in_dim.67
  35.5 0.0 copy-start.1
  35.5 0.0 copy-start.3
  35.5 6.2 %while.18 = (s32[]{:T(128)}, f32[2,256]{1,0:T(2,128)S(1)}, f32[2,256]{1,0:T(2,128)S(1)}, f32[256,2,128]{0,2,1:T(8,128)}, s32[]{:T(128)}, /*index=5*/bf16[2048,25...) while((s32[]{:T(128)}, f32[2,256]{1,0:T(2,128)S(1)}, ...), condition=%wide.region_6.7_spmd.clone, body=%wide.region_1.6_spmd.clone.sunk | while | flops 610142976 | bytes 23441912 | solution.py:624
  35.5 6.2 %conditional.3 = ((f32[2,256]{1,0:T(2,128)S(1)}, f32[2,256]{1,0:T(2,128)S(1)}, f32[256,2,128]{0,2,1:T(8,128)})) conditional(s32[]{:T(128)} %convert_element_type.97, (f32[2,256]{1,0:T(2,128)S(1)}, f32[2,256]{1,0:T(2,128)S(1)}, f32[256,2,128]{0,2,1:T(8,128)}) %tuple.61, (s32[]{:T(128)}, s32[]{:T(128)}, bf16[2048,256]{1,0:T(8,128)(2,1)}, ...), branch_computations={%region_2.0_spmd, %region_3.5_spmd} | conditional | flops 610142976 | bytes 23440610 | solution.py:622
  35.5 0.0 copy-start.5
  35.5 0.0 copy-start.6
  35.6 1.6 %convolution_convert_fusion.1 = bf16[1024,256]{0,1:T(8,128)(2,1)S(1)} fusion(bf16[256,256]{1,0:T(8,128)(2,1)} %get-tuple-element.320, bf16[2048,256]{1,0:T(8,128)(2,1)} %get-tuple-element.319, s32[]{:T(128)S(6)} %select_n.26), kind=kOutput, calls=%fused_computation.8 | convolution fusion | flops 134479872 | bytes 1179652 | tf_op jit(solution)/shard_map/while/body/eval_jaxpr/cond/branch_1_fun/dot_general | solution.py:582
  37.1 1.4 %fusion.33 = f32[2,1024,256]{2,1,0:T(8,128)S(1)} fusion(bf16[1024,2,128]{0,2,1:T(8,128)(2,1)S(1)} %bitcast.39, bf16[256,2,128]{2,0,1:T(8,128)(2,1)} %get-tuple-element.321), kind=kOutput, calls=%fused_computation.64 | convolution fusion | flops 134217728 | bytes 2752512 | tf_op jit(solution)/shard_map/while/body/eval_jaxpr/cond/branch_1_fun/qhd,khd->hqk/dot_general | solution.py:591
  38.5 0.2 broadcast_compare_fusion
  38.8 0.0 copy-start.7
  38.8 0.6 fusion.32
  39.4 0.6 copy-done.4
  40.0 0.3 convolution_convert_fusion
  40.4 0.6 fusion.6
  40.9 0.0 copy-start.8
  40.9 0.4 fusion.5
  41.4 0.3 copy-done.8
  41.7 1.6 %divide_convert_fusion = bf16[256,2,128]{0,2,1:T(8,128)(2,1)} fusion(f32[256,2,128]{0,2,1:T(8,128)} %get-tuple-element.345, f32[256,2]{0,1:T(2,128)S(1)} %bitcast.48), kind=kLoop, calls=%fused_computation.33 | loop fusion | flops 131072 | bytes 395264 | tf_op jit(solution)/shard_map/convert_element_type | solution.py:625
  43.3 1.0 copy.57.heads_ref
  44.4 0.7 select_reduce_fusion
  45.1 0.6 pad_maximum_fusion.3
  45.7 0.8 copy.54
  46.5 0.7 reshape.213.gain_ref
  47.2 0.0 copy-start.2
  47.2 1.2 copy-done.2
  48.4 78.3 %layer_tail.1 = bf16[64,2048]{1,0:T(8,128)(2,1)S(1)} custom-call(bf16[256,256]{1,0:T(8,128)(2,1)S(1)} %copy.57.heads_ref, bf16[256,2048]{1,0:T(8,128)(2,1)S(1)} %copy-done.2, bf16[64,2048]{1,0:T(8,128)(2,1)S(1)} %copy-done.3, bf16[1,2048]{1,0:T(2,128)(2,1)S(1)} %reshape.213.gain_ref, bf16[64,128]{1,0:T(8,128)(2,1)S(1)} %pad.5.route_ref, ...), custom_call_target="tpu_custom_call" | custom-call | tf_op jit(solution)/shard_map/layer_tail/pallas_call | solution.py:566
  126.8 0.7 copy.79
  (28 shorter events, 0.1 us)
Async XLA Ops:
  27.8 6.1 %copy-start.9 = (bf16[256,256]{1,0:T(8,128)(2,1)S(1)}, bf16[256,256]{1,0:T(8,128)(2,1)}, u32[]{:S(2)}) copy-start(bf16[256,256]{1,0:T(8,128)(2,1)} %param.22) | copy-start | bytes 393220
  35.4 8.9 %copy-start.10 = (f32[64,4]{0,1:T(4,128)S(1)}, f32[64,4]{0,1:T(4,128)}, u32[]{:S(2)}) copy-start(f32[64,4]{0,1:T(4,128)} %param.33) | copy-start | bytes 3076
  35.4 11.7 %copy-start = (bf16[1,2048,384]{2,1,0:T(8,128)(2,1)S(1)}, bf16[1,2048,384]{2,1,0:T(8,128)(2,1)}, u32[]{:S(2)}) copy-start(bf16[1,2048,384]{2,1,0:T(8,128)(2,1)} %eg_hbm.1) | copy-start | bytes 4718596
  35.5 11.7 %copy-start.1 = (bf16[1,2048,384]{2,1,0:T(8,128)(2,1)S(1)}, bf16[1,2048,384]{2,1,0:T(8,128)(2,1)}, u32[]{:S(2)}) copy-start(bf16[1,2048,384]{2,1,0:T(8,128)(2,1)} %eu_hbm.1) | copy-start | bytes 4718596
  35.5 11.7 %copy-start.3 = (bf16[64,2048]{1,0:T(8,128)(2,1)S(1)}, bf16[64,2048]{1,0:T(8,128)(2,1)}, u32[]{:S(2)}) copy-start(bf16[64,2048]{1,0:T(8,128)(2,1)} %resid_ref.1) | copy-start | bytes 786436
  35.5 3.2 %copy-start.5 = (bf16[2048,64]{0,1:T(8,128)(2,1)S(1)}, bf16[2048,64]{0,1:T(8,128)(2,1)}, u32[]{:S(2)}) copy-start(bf16[2048,64]{0,1:T(8,128)(2,1)} %get-tuple-element.322) | copy-start | bytes 786436 | tf_op jit(solution)/shard_map/while/body/eval_jaxpr/cond
  35.5 3.2 %copy-start.6 = (bf16[256,2,64]{0,2,1:T(8,128)(2,1)S(1)}, bf16[256,2,64]{0,2,1:T(8,128)(2,1)}, u32[]{:S(2)}) copy-start(bf16[256,2,64]{0,2,1:T(8,128)(2,1)} %get-tuple-element.323) | copy-start | bytes 196612 | tf_op jit(solution)/shard_map/while/body/eval_jaxpr/cond
  38.8 1.2 copy-start.4
  38.8 1.6 %copy-start.7 = (f32[256,2,128]{0,2,1:T(8,128)S(1)}, f32[256,2,128]{0,2,1:T(8,128)}, u32[]{:S(2)}) copy-start(f32[256,2,128]{0,2,1:T(8,128)} %get-tuple-element.325) | copy-start | bytes 786436 | tf_op jit(solution)/shard_map/while/body/eval_jaxpr/cond
  40.9 0.7 copy-start.8
  47.2 1.2 copy-start.2

commit v2 on v0

--- a/solution.py
+++ b/solution.py
@@ -1,8 +1,12 @@
+import functools
 import math
 
 import jax
 import jax.numpy as jnp
+import numpy as np
 from jax import lax
+from jax.experimental import pallas as pl
+from jax.experimental.pallas import tpu as pltpu
 from jax.sharding import PartitionSpec as P
 
 NOPE = 128
@@ -38,7 +42,7 @@
     ).astype(jnp.bfloat16)
 
 
-def body(
+def start_body(
     query_nope,
     query_rope,
     latent,
@@ -200,6 +204,463 @@
     ).astype(jnp.bfloat16)
 
 
+MESH = pl.DeviceIdType.MESH
+F32 = jnp.float32
+BF16 = jnp.bfloat16
+LANES = 128
+
+
+def arrived(ref, sem):
+    pltpu.make_async_copy(ref, ref, sem).wait()
+
+
+def greet(z, depth, me, tp_peers):
+    barrier = pltpu.get_barrier_semaphore()
+
+    @pl.when(z + 1 < depth)
+    def _():
+        pl.semaphore_signal(barrier, inc=1, device_id={"sp": me + 2}, device_id_type=MESH)
+
+    @pl.when(z > 0)
+    def _():
+        pl.semaphore_signal(barrier, inc=1, device_id={"sp": me - 2}, device_id_type=MESH)
+
+    pair = z * 4 + 1 - me
+    pl.semaphore_signal(barrier, inc=1, device_id={"sp": pair}, device_id_type=MESH)
+    for peer in tp_peers:
+        pl.semaphore_signal(barrier, inc=1, device_id={"tp": peer}, device_id_type=MESH)
+    line_peers = (z + 1 < depth).astype(jnp.int32) + (z > 0).astype(jnp.int32)
+    pl.semaphore_wait(barrier, 1 + len(tp_peers) + line_peers)
+
+
+class Gather:
+    def __init__(self, view, chunks, up, down, side, got, z, x, depth, relay=None):
+        self.view, self.up, self.down, self.side, self.got = view, up, down, side, got
+        self.z, self.x, self.depth, self.chunks = z, x, depth, chunks
+        self.relay = relay if relay is not None else (lambda block, ch: None)
+        self.me = z * 2 + x
+
+    def copy(self, block, ch, sem, to):
+        return pltpu.make_async_remote_copy(
+            src_ref=self.view(block, ch), dst_ref=self.view(block, ch), send_sem=sem,
+            recv_sem=self.got.at[block, ch], device_id={"sp": to}, device_id_type=MESH)
+
+    def send_up(self, zz, ch):
+        return self.copy(zz * 2 + self.x, ch, self.up.at[zz, ch], self.me + 2)
+
+    def send_down(self, zz, ch):
+        return self.copy(zz * 2 + self.x, ch, self.down.at[zz, ch], self.me - 2)
+
+    def send_side(self, zz, ch):
+        return self.copy(zz * 2 + self.x, ch, self.side.at[zz, ch], self.z * 2 + 1 - self.x)
+
+    def take(self, block, ch):
+        arrived(self.view(block, ch), self.got.at[block, ch])
+
+    def start(self):
+        z = self.z
+        for ch in range(self.chunks):
+            @pl.when(z + 1 < self.depth)
+            def _():
+                self.send_up(z, ch).start()
+
+            @pl.when(z > 0)
+            def _():
+                self.send_down(z, ch).start()
+
+            self.send_side(z, ch).start()
+
+    def run(self):
+        z, x, depth = self.z, self.x, self.depth
+        for j in range(1, depth):
+            for ch in range(self.chunks):
+                @pl.when(z - j >= 0)
+                def _():
+                    zz = z - j
+                    self.take(zz * 2 + x, ch)
+
+                    @pl.when(z + 1 < depth)
+                    def _():
+                        self.send_up(zz, ch).start()
+
+                    self.send_side(zz, ch).start()
+                    self.relay(zz * 2 + x, ch)
+
+                @pl.when(z + j < depth)
+                def _():
+                    zz = z + j
+                    self.take(zz * 2 + x, ch)
+
+                    @pl.when(z > 0)
+                    def _():
+                        self.send_down(zz, ch).start()
+
+                    self.send_side(zz, ch).start()
+                    self.relay(zz * 2 + x, ch)
+
+        def crossed(zz):
+            block = zz * 2 + 1 - x
+            for ch in range(self.chunks):
+                self.take(block, ch)
+                self.relay(block, ch)
+
+        crossed(z)
+        for j in range(1, depth):
+            @pl.when(z - j >= 0)
+            def _():
+                crossed(z - j)
+
+            @pl.when(z + j < depth)
+            def _():
+                crossed(z + j)
+
+    def finish(self):
+        z, depth = self.z, self.depth
+        for zz in range(depth):
+            for ch in range(self.chunks):
+                @pl.when((zz <= z) & (z + 1 < depth))
+                def _():
+                    self.send_up(zz, ch).wait_send()
+
+                @pl.when((zz >= z) & (z > 0))
+                def _():
+                    self.send_down(zz, ch).wait_send()
+
+                self.send_side(zz, ch).wait_send()
+
+
+def gated(rows, gate, up, down):
+    gate_part = jnp.dot(rows, gate[...], preferred_element_type=F32)
+    upper = jnp.dot(rows, up[...], preferred_element_type=F32)
+    hidden = (gate_part / (1.0 + jnp.exp(-gate_part)) * upper).astype(BF16)
+    return jnp.dot(hidden, down[...], preferred_element_type=F32).astype(BF16)
+
+
+CHUNKS = 2
+
+
+def rotated(values, cosine, sine):
+    lane = lax.broadcasted_iota(jnp.int32, values.shape, 1)
+    half = ROPE // 2
+    swapped = jnp.where(lane % ROPE < half, pltpu.roll(values, LANES - half, 1), pltpu.roll(values, half, 1))
+    return values * cosine + swapped * sine
+
+
+def layer_kernel(depth, chips, experts,
+                 nope_ref, rope_ref, latent_ref, key_ref, latent_gain_ref, resid_ref, gain_ref, ids_ref, route_ref,
+                 table_hbm, kup_hbm, vup_hbm, proj_hbm, eg_hbm, eu_hbm, ed_hbm, sg_hbm, su_hbm, sd_hbm,
+                 out_ref,
+                 table, kup, vup, proj_ref, eg, eu, ed, sg, su, sd, load_sem,
+                 lat, query, heads_ref, mixed, l_up, l_down, l_side, l_got, relay_out, relay_in,
+                 part, sib, ysend, yrecv, sib_s, sib_r, y_s, y_r,
+                 hid, shared, xbuf, up, down, side, got,
+                 contrib, xr, upr, dnr, rx_s, rx_r, rz_s, up_r, dn_r):
+    me = lax.axis_index("sp")
+    t = lax.axis_index("tp")
+    z, x = me // 2, me % 2
+    y, c = t // 2, t % 2
+    tokens, width = resid_ref.shape
+    rows, rank = latent_ref.shape
+    head_cols = nope_ref.shape[1]
+    local_heads = head_cols // NOPE
+    columns = pl.ds(pl.multiple_of(t * head_cols, head_cols), head_cols)
+    loads = [pltpu.make_async_copy(src, dst, load_sem.at[i]) for i, (src, dst) in enumerate(
+        ((table_hbm.at[pl.ds(pl.multiple_of(me * rows, rows), rows)], table),
+         (kup_hbm.at[:, columns], kup), (vup_hbm.at[:, columns], vup), (proj_hbm, proj_ref),
+         (sg_hbm, sg), (su_hbm, su), (sd_hbm, sd), (eg_hbm.at[0], eg), (eu_hbm.at[0], eu), (ed_hbm.at[0], ed)))]
+    for load in loads:
+        load.start()
+    sibling = t + 1 - 2 * c
+    peers = [lax.rem(t + 2 * d, 2 * chips) for d in range(1, chips)]
+    greet(z, depth, me, [sibling] + peers)
+
+    wide = latent_ref[...].astype(F32)
+    factor = lax.rsqrt(jnp.mean(wide * wide, axis=-1, keepdims=True) + norm_eps)
+    lat[me, :, :rank] = (wide * factor * latent_gain_ref[...].astype(F32)).astype(BF16)
+    loads[0].wait()
+    cosine, sine = table[:, :ROPE], table[:, ROPE:]
+    cosine = jnp.concatenate([cosine, cosine], axis=1)
+    sine = jnp.concatenate([sine, sine], axis=1)
+    key = key_ref[...].astype(F32)
+    lat[me, :, rank:] = rotated(jnp.concatenate([key, key], axis=1), cosine, sine).astype(BF16)
+
+    half_rows = rows // 2
+
+    def half_view(block, half):
+        return lat.at[block, pl.ds(pl.multiple_of(half * half_rows, half_rows), half_rows)]
+
+    def relay_copy(block):
+        return pltpu.make_async_remote_copy(
+            src_ref=half_view(block, c), dst_ref=half_view(block, c),
+            send_sem=relay_out.at[block], recv_sem=relay_in.at[block],
+            device_id={"tp": sibling}, device_id_type=MESH)
+
+    latents = Gather(lambda b, ch: half_view(b, c), 1, l_up, l_down, l_side, l_got, z, x, depth,
+                     relay=lambda b, ch: relay_copy(b).start())
+    latents.start()
+    lane = lax.broadcasted_iota(jnp.int32, (rows, LANES), 1)
+    turned = rotated(rope_ref[...].astype(F32), cosine, sine)
+    for h in range(local_heads):
+        query[h, :, :NOPE] = nope_ref[:, h * NOPE:(h + 1) * NOPE]
+        query[h, :, NOPE:] = jnp.where(lane // ROPE == h, turned, 0.0).astype(BF16)
+    lane = lax.broadcasted_iota(jnp.int32, (tokens, LANES), 1)
+    dense = jnp.zeros((tokens, LANES), F32)
+    for k in range(ids_ref.shape[1]):
+        dense = dense + jnp.where(lane % experts == ids_ref[:, k:k + 1], route_ref[:, k:k + 1], 0.0)
+    coarse = dense.astype(BF16).astype(F32)
+    terms = jnp.where(lane < experts, coarse, jnp.where(lane < 2 * experts, dense - coarse, 0.0))
+    xbuf[me, :, width:] = terms.astype(BF16)
+    loads[1].wait()
+    loads[2].wait()
+    value_t = vup[...].astype(F32).T.astype(BF16)
+    vup[...] = value_t
+    latents.run()
+    for block in range(2 * depth):
+        @pl.when(block != me)
+        def _():
+            arrived(half_view(block, 1 - c), relay_in.at[block])
+
+    span = 2 * rows
+    score_scale = 1.0 / math.sqrt(NOPE + ROPE)
+    mixed[...] = jnp.zeros(mixed.shape, F32)
+
+    def attend(zz, state):
+        pair = lat[pl.ds(zz * 2, 2)].reshape(span, rank + LANES)
+        keys = jnp.dot(pair[:, :rank], kup[...], preferred_element_type=F32).astype(BF16)
+        values_t = lax.dot_general(
+            vup[...], pair[:, :rank], (((1,), (1,)), ((), ())), preferred_element_type=F32).astype(BF16)
+        key_pos = zz * span + lax.broadcasted_iota(jnp.int32, (span, rows), 0)
+        query_pos = me * rows + lax.broadcasted_iota(jnp.int32, (span, rows), 1)
+        allowed = key_pos <= query_pos
+        fresh = []
+        for h in range(local_heads):
+            top, weight_sum = state[h]
+            full = jnp.concatenate([keys[:, h * NOPE:(h + 1) * NOPE], pair[:, rank:]], axis=1)
+            scores = lax.dot_general(
+                full, query[h], (((1,), (1,)), ((), ())), preferred_element_type=F32) * score_scale
+            scores = jnp.where(allowed, scores, -1e30)
+            newest = jnp.maximum(top, jnp.max(scores, axis=0, keepdims=True))
+            weights = jnp.exp(scores - newest)
+            shrink = jnp.exp(top - newest)
+            weight_sum = weight_sum * shrink + jnp.sum(weights, axis=0, keepdims=True)
+            mixed[h] = mixed[h] * shrink + jnp.dot(
+                values_t[h * VDIM:(h + 1) * VDIM], weights.astype(BF16), preferred_element_type=F32)
+            fresh.append((newest, weight_sum))
+        return tuple(fresh)
+
+    first = tuple((jnp.full((1, rows), -1e30, F32), jnp.zeros((1, rows), F32)) for _ in range(local_heads))
+    folded = lax.fori_loop(0, z + 1, attend, first)
+    for h in range(local_heads):
+        heads_ref[:, h * VDIM:(h + 1) * VDIM] = (mixed[h] / folded[h][1]).T.astype(BF16)
+    loads[3].wait()
+
+    def project(block):
+        mine = heads_ref[pl.ds(pl.multiple_of(block * tokens, tokens), tokens), :]
+        return jnp.dot(mine, proj_ref[...], preferred_element_type=F32).astype(BF16)
+
+    def to_sibling(yy):
+        return pltpu.make_async_remote_copy(
+            src_ref=part.at[yy], dst_ref=sib.at[yy], send_sem=sib_s.at[yy], recv_sem=sib_r.at[yy],
+            device_id={"tp": sibling}, device_id_type=MESH)
+
+    def to_chip(d):
+        return pltpu.make_async_remote_copy(
+            src_ref=ysend.at[d - 1], dst_ref=yrecv.at[d - 1], send_sem=y_s.at[d - 1], recv_sem=y_r.at[d - 1],
+            device_id={"tp": peers[d - 1]}, device_id_type=MESH)
+
+    ahead = [lax.rem(y + d, chips) for d in range(1, chips)] + [y]
+    for yy in ahead:
+        part[yy] = project(yy * 2 + 1 - c)
+        to_sibling(yy).start()
+    for d in range(1, chips):
+        yy = ahead[d - 1]
+        mine = project(yy * 2 + c).astype(F32)
+        arrived(sib.at[yy], sib_r.at[yy])
+        ysend[d - 1] = (mine + sib[yy].astype(F32)).astype(BF16)
+        to_chip(d).start()
+    total = project(y * 2 + c).astype(F32)
+    arrived(sib.at[y], sib_r.at[y])
+    total = total + sib[y].astype(F32)
+    for d in range(1, chips):
+        arrived(yrecv.at[d - 1], y_r.at[d - 1])
+        total = total + yrecv[d - 1].astype(F32)
+    hidden_one = (resid_ref[...].astype(F32) + total).astype(BF16)
+    hid[...] = hidden_one
+    wide = hidden_one.astype(F32)
+    factor = lax.rsqrt(jnp.mean(wide * wide, axis=-1, keepdims=True) + norm_eps)
+    xbuf[me, :, :width] = (wide * factor * gain_ref[...].astype(F32)).astype(BF16)
+
+    piece = tokens // CHUNKS
+    ring = Gather(lambda b, ch: xbuf.at[b, pl.ds(ch * piece, piece)], CHUNKS, up, down, side, got, z, x, depth)
+    ring.start()
+    for load in loads[4:7]:
+        load.wait()
+    shared[...] = gated(xbuf[me, :, :width], sg, su, sd)
+    ring.run()
+    for load in loads[7:]:
+        load.wait()
+
+    def cross(zz, ch):
+        return pltpu.make_async_remote_copy(
+            src_ref=contrib.at[zz, 1 - x, pl.ds(ch * piece, piece)], dst_ref=xr.at[zz, pl.ds(ch * piece, piece)],
+            send_sem=rx_s.at[zz, ch], recv_sem=rx_r.at[zz, ch],
+            device_id={"sp": z * 2 + 1 - x}, device_id_type=MESH)
+
+    high = (z >= depth // 2).astype(jnp.int32)
+
+    def expert_step(j, carry):
+        pick = high * j + (1 - high) * (depth - 2 - j)
+        pick = pick + (pick >= z).astype(jnp.int32)
+        last = (j == depth - 1).astype(jnp.int32)
+        zz = last * z + (1 - last) * pick
+        pair = xbuf[pl.ds(zz * 2, 2)].reshape(2 * tokens, width + LANES)
+        routes = pair[:, width:].astype(F32)
+        lane = lax.broadcasted_iota(jnp.int32, routes.shape, 1)
+        weight = jnp.sum(jnp.where((lane == me) | (lane == me + experts), routes, 0.0), axis=1, keepdims=True)
+        answer = gated(pair[:, :width], eg, eu, ed).astype(F32) * weight
+        contrib[zz] = answer.astype(BF16).reshape(2, tokens, width)
+        for ch in range(CHUNKS):
+            cross(zz, ch).start()
+        return carry
+
+    lax.fori_loop(0, depth, expert_step, 0)
+
+    def pass_on(dst, ch, landing, recv, to):
+        return pltpu.make_async_remote_copy(
+            src_ref=contrib.at[dst, x, pl.ds(ch * piece, piece)], dst_ref=landing.at[dst, pl.ds(ch * piece, piece)],
+            send_sem=rz_s.at[dst, ch], recv_sem=recv.at[dst, ch],
+            device_id={"sp": to}, device_id_type=MESH)
+
+    def local_sum(dst, ch):
+        here = pl.ds(ch * piece, piece)
+        arrived(xr.at[dst, here], rx_r.at[dst, ch])
+        return contrib[dst, x, here].astype(F32) + xr[dst, here].astype(F32)
+
+    def hop(dst, ch, landing, recv, at_end, to):
+        here = pl.ds(ch * piece, piece)
+
+        @pl.when(jnp.logical_not(at_end))
+        def _():
+            partial = local_sum(dst, ch)
+            arrived(landing.at[dst, here], recv.at[dst, ch])
+            contrib[dst, x, here] = (partial + landing[dst, here].astype(F32)).astype(BF16)
+
+        @pl.when(at_end)
+        def _():
+            contrib[dst, x, here] = local_sum(dst, ch).astype(BF16)
+
+        pass_on(dst, ch, landing, recv, to).start()
+
+    for k in range(depth - 1):
+        for ch in range(CHUNKS):
+            @pl.when(depth - 1 - k > z)
+            def _():
+                hop(depth - 1 - k, ch, upr, up_r, z == 0, me + 2)
+
+            @pl.when(k < z)
+            def _():
+                hop(k, ch, dnr, dn_r, z + 1 == depth, me - 2)
+
+    @pl.when(z == 0)
+    def _():
+        upr[z] = jnp.zeros(upr.shape[1:], BF16)
+
+    @pl.when(z + 1 == depth)
+    def _():
+        dnr[z] = jnp.zeros(dnr.shape[1:], BF16)
+
+    for ch in range(CHUNKS):
+        here = pl.ds(ch * piece, piece)
+
+        @pl.when(z > 0)
+        def _():
+            arrived(upr.at[z, here], up_r.at[z, ch])
+
+        @pl.when(z + 1 < depth)
+        def _():
+            arrived(dnr.at[z, here], dn_r.at[z, ch])
+
+        routed = (local_sum(z, ch) + upr[z, here].astype(F32) + dnr[z, here].astype(F32)).astype(BF16)
+        out_ref[here] = (hid[here].astype(F32) + routed.astype(F32) + shared[here].astype(F32)).astype(BF16)
+
+    latents.finish()
+    for block in range(2 * depth):
+        @pl.when(block != me)
+        def _():
+            relay_copy(block).wait_send()
+    for yy in range(chips):
+        to_sibling(yy).wait_send()
+    for d in range(1, chips):
+        to_chip(d).wait_send()
+    ring.finish()
+    for zz in range(depth):
+        for ch in range(CHUNKS):
+            cross(zz, ch).wait_send()
+
+            @pl.when(zz != z)
+            def _():
+                arrived(contrib.at[zz, x, pl.ds(ch * piece, piece)], rz_s.at[zz, ch])
+
+
+def line_body(query_nope, query_rope, latent, key_rope, latent_gain, key_up, value_up, out_proj, residual, ffn_gain,
+              expert_ids, route_weights, expert_gate, expert_up, expert_down, shared_gate, shared_up, shared_down):
+    sp, tp = lax.axis_size("sp"), lax.axis_size("tp")
+    depth, chips = sp // 2, tp // 2
+    rows, rank = latent.shape
+    tokens, width = residual.shape
+    ff = shared_gate.shape[1]
+    head_cols = query_nope.shape[1]
+    half_dim = ROPE // 2
+    frequency = np.float32(rope_base) ** (-np.arange(half_dim, dtype=np.float32) / np.float32(half_dim))
+    angles = np.arange(sp * rows, dtype=np.float32)[:, None] * frequency[None, :]
+    cosine, sine = np.cos(angles), np.sin(angles)
+    table = jnp.asarray(np.concatenate([cosine, cosine, -sine, sine], axis=1), F32)
+    dma = pltpu.SemaphoreType.DMA
+    vmem = pl.BlockSpec(memory_space=pltpu.VMEM)
+    hbm = pl.BlockSpec(memory_space=pl.ANY)
+    block = (tokens, width)
+
+    def buf(*shape):
+        return pltpu.VMEM(shape, BF16)
+
+    scratch = [
+        pltpu.VMEM((rows, 2 * ROPE), F32), buf(rank, head_cols), buf(rank, head_cols), buf(head_cols, width),
+        buf(width, ff), buf(width, ff), buf(ff, width), buf(width, ff), buf(width, ff), buf(ff, width), dma((10,)),
+        buf(sp, rows, rank + LANES), buf(head_cols // NOPE, rows, NOPE + LANES), buf(rows, head_cols),
+        pltpu.VMEM((head_cols // VDIM, VDIM, rows), F32),
+        dma((depth, 1)), dma((depth, 1)), dma((depth, 1)), dma((sp, 1)), dma((sp,)), dma((sp,)),
+        buf(chips, *block), buf(chips, *block), buf(chips - 1, *block), buf(chips - 1, *block),
+        dma((chips,)), dma((chips,)), dma((chips - 1,)), dma((chips - 1,)),
+        buf(*block), buf(*block), buf(sp, tokens, width + LANES),
+        dma((depth, CHUNKS)), dma((depth, CHUNKS)), dma((depth, CHUNKS)), dma((sp, CHUNKS)),
+        buf(depth, 2, *block), buf(depth, *block), buf(depth, *block), buf(depth, *block),
+    ] + [dma((depth, CHUNKS))] * 5
+    return pl.pallas_call(
+        functools.partial(layer_kernel, depth, chips, sp),
+        out_shape=jax.ShapeDtypeStruct(block, BF16),
+        in_specs=[vmem] * 9 + [hbm] * 10,
+        out_specs=vmem,
+        scratch_shapes=scratch,
+        compiler_params=pltpu.CompilerParams(
+            collective_id=0, has_side_effects=True, vmem_limit_bytes=48 * 1024 * 1024),
+        name="layer",
+    )(query_nope, query_rope, latent, key_rope, latent_gain.reshape(1, -1), residual, ffn_gain.reshape(1, -1),
+      expert_ids, route_weights, table, key_up, value_up, out_proj,
+      expert_gate, expert_up, expert_down, shared_gate, shared_up, shared_down)
+
+
+def body(*args):
+    latent, residual, expert_ids, expert_gate = args[2], args[8], args[10], args[12]
+    sp, tp = lax.axis_size("sp"), lax.axis_size("tp")
+    tokens, slots = residual.shape[0], expert_ids.shape[1]
+    experts = expert_gate.shape[0] * sp
+    capacity = 2 * tokens * slots // experts
+    dense = capacity >= tokens and expert_gate.shape[0] == 1 and args[0].shape[1] == 2 * NOPE == latent.shape[1]
+    if dense and sp % 2 == 0 and tp % 2 == 0 and tp > 2 and 2 * sp <= LANES:
+        return line_body(*args)
+    return start_body(*args)
+
+
 def solution(mesh):
     in_specs = (
         P("sp", "tp"),

time: 231 us -> 105 us (0.45)
  Pallas kernels: 0 us -> 90.6 us
  blocking collectives: 86.8 us -> 0 us
  waiting for transfers between devices: 77.7 us -> 0 us
  matrix products: 17.1 us -> 0 us
  between operations: 13.7 us -> 0.03 us
  other arithmetic: 12.5 us -> 0 us
  starting transfers between devices: 4.73 us -> 0 us
  local copies, waits for them, and re-layouts: 17.5 us -> 14 us
    pallas_call x0 -> x1, Pallas kernels: none -> 90.6 us  [line_body(): pl.pallas_call(functools.partial(layer_kernel, depth, chips, sp), out_sha...]
    all_to_all x1 -> x0, blocking collectives: 53.7 us -> none  [body(): lax.all_to_all(outgoing, 'sp', split_axis=0, concat_axis=0, tiled=True)]
    all_to_all x1 -> x0, waiting for transfers between devices: 45.3 us -> none  [body(): lax.all_to_all(answered, 'sp', split_axis=0, concat_axis=0, tiled=True)]
    all_gather x1 -> x0, blocking collectives: 33.1 us -> none  [body(): lax.all_gather(rot_key, 'sp', axis=0, tiled=True)]
    reduce_scatter x1 -> x0, waiting for transfers between devices: 25.8 us -> none  [body(): lax.psum_scatter(jnp.dot(heads_out, out_proj, preferred_element_type=jnp....]
    dot_general x10 -> x0, matrix products: 17.1 us -> none  [the longest x1 5.77 us: body(): jnp.einsum('seif,efd->seid', expert_hidden, expert_down, preferred_elemen...]
    unnamed x22, local copies, waits for them, and re-layouts: 2.65 us -> 12.6 us
    gather x2 -> x0, local copies, waits for them, and re-layouts: 7.57 us -> none  [the longest x1 4.22 us: body(): picked = returned.reshape(experts * capacity, model_width)[target]]
  transfers between devices with their start and end apart: 3 -> 0, of which waited for: 3 -> 0; matrix products, arithmetic and copies ran while one was open for 4% -> 0% of each run, Pallas kernels for 0% -> 0%
where the time goes in v2:
time: 105 us
  Pallas kernels  90.6 us (86%)
  local copies, waits for them, and re-layouts  14 us (13%)
    pallas_call x1, Pallas kernels, line_body(): pl.pallas_call(functools.partial(layer_kernel, depth, chips, sp), out_sha...  90.6 us
    unnamed x22, local copies, waits for them, and re-layouts  12.6 us

profile of v2, /device:TPU:0, one launch (start us, length us, event | category | flops | bytes accessed | tf_op | source)
XLA Modules:
  0.0 104.6 jit_solution(7714497965924735444)
XLA Ops:
  0.0 0.7 reshape.6.latent_gain_ref
  0.7 0.7 reshape.7.gain_ref
  1.4 0.8 copy.21.ids_ref
  2.1 0.8 copy.22.route_ref
  2.9 0.9 copy.20.key_ref
  3.8 0.0 copy-start
  3.8 1.4 %copy-done = bf16[1,2048,384]{2,1,0:T(8,128)(2,1)S(1)} copy-done((bf16[1,2048,384]{2,1,0:T(8,128)(2,1)S(1)}, bf16[1,2048,384]{2,1,0:T(8,128)(2,1)}, u32[]{:S(2)}) %copy-start) | copy-done | bytes 1572888
  5.2 0.0 copy-start.1
  5.2 1.2 %copy-done.1 = bf16[256,2048]{1,0:T(8,128)(2,1)S(1)} copy-done((bf16[256,2048]{1,0:T(8,128)(2,1)S(1)}, bf16[256,2048]{1,0:T(8,128)(2,1)}, u32[]{:S(2)}) %copy-start.1) | copy-done | bytes 1048600
  6.4 0.0 copy-start.2
  6.4 1.2 %copy-done.2 = f32[2048,128]{1,0:T(8,128)S(1)} copy-done((f32[2048,128]{1,0:T(8,128)S(1)}, f32[2048,128]{1,0:T(8,128)}, u32[]{:S(2)}) %copy-start.2) | copy-done | bytes 1048600
  7.6 0.0 copy-start.3
  7.6 1.0 copy-done.3
  8.7 0.0 copy-start.4
  8.7 1.0 copy-done.4
  9.7 0.0 copy-start.5
  9.7 0.9 copy-done.5
  10.7 0.0 copy-start.6
  10.7 0.9 copy-done.6
  11.6 0.0 copy-start.7
  11.6 0.9 copy-done.7
  12.5 0.0 copy-start.8
  12.5 0.8 copy-done.8
  13.3 90.6 %layer.1 = bf16[64,2048]{1,0:T(8,128)(2,1)S(1)} custom-call(bf16[256,256]{1,0:T(8,128)(2,1)S(1)} %copy-done.6, bf16[256,128]{1,0:T(8,128)(2,1)S(1)} %copy-done.8, bf16[256,256]{1,0:T(8,128)(2,1)S(1)} %copy-done.7, bf16[256,64]{1,0:T(8,128)(2,1)S(1)} %copy.20.key_ref, bf16[1,256]{1,0:T(2,128)(2,1)S(1)} %reshape.6.latent_gain_ref, ...), custom_call_target="tpu_custom_call" | custom-call | tf_op jit(solution)/shard_map/layer/pallas_call | solution.py:638
  103.9 0.7 copy.24
Async XLA Ops:
  3.8 1.4 %copy-start = (bf16[1,2048,384]{2,1,0:T(8,128)(2,1)S(1)}, bf16[1,2048,384]{2,1,0:T(8,128)(2,1)}, u32[]{:S(2)}) copy-start(bf16[1,2048,384]{2,1,0:T(8,128)(2,1)} %eg_hbm.1) | copy-start | bytes 4718596
  5.2 1.2 %copy-start.1 = (bf16[256,2048]{1,0:T(8,128)(2,1)S(1)}, bf16[256,2048]{1,0:T(8,128)(2,1)}, u32[]{:S(2)}) copy-start(bf16[256,2048]{1,0:T(8,128)(2,1)} %proj_hbm.1) | copy-start | bytes 3145732
  6.4 1.2 %copy-start.2 = (f32[2048,128]{1,0:T(8,128)S(1)}, f32[2048,128]{1,0:T(8,128)}, u32[]{:S(2)}) copy-start(f32[2048,128]{1,0:T(8,128)} %constant.2.clone.table_hbm) | copy-start | bytes 3145732
  7.6 1.0 copy-start.3
  8.7 1.0 copy-start.4
  9.7 0.9 copy-start.5
  10.7 0.9 copy-start.6
  11.6 0.9 copy-start.7
  12.5 0.8 copy-start.8

commit v3 on v2

--- a/solution.py
+++ b/solution.py
@@ -257,20 +257,20 @@
     def take(self, block, ch):
         arrived(self.view(block, ch), self.got.at[block, ch])
 
-    def start(self):
+    def start(self, ch):
         z = self.z
-        for ch in range(self.chunks):
-            @pl.when(z + 1 < self.depth)
-            def _():
-                self.send_up(z, ch).start()
-
-            @pl.when(z > 0)
-            def _():
-                self.send_down(z, ch).start()
-
-            self.send_side(z, ch).start()
-
-    def run(self):
+
+        @pl.when(z + 1 < self.depth)
+        def _():
+            self.send_up(z, ch).start()
+
+        @pl.when(z > 0)
+        def _():
+            self.send_down(z, ch).start()
+
+        self.send_side(z, ch).start()
+
+    def run(self, ready=None):
         z, x, depth = self.z, self.x, self.depth
         for j in range(1, depth):
             for ch in range(self.chunks):
@@ -298,17 +298,28 @@
                     self.send_side(zz, ch).start()
                     self.relay(zz * 2 + x, ch)
 
+            if ready is not None:
+                @pl.when(z - j + 1 >= 0)
+                def _():
+                    ready(z - j + 1, j == 1)
+
         def crossed(zz):
             block = zz * 2 + 1 - x
             for ch in range(self.chunks):
                 self.take(block, ch)
                 self.relay(block, ch)
 
-        crossed(z)
+        if ready is not None:
+            @pl.when(z - depth + 1 >= 0)
+            def _():
+                ready(z - depth + 1, False)
+        else:
+            crossed(z)
         for j in range(1, depth):
-            @pl.when(z - j >= 0)
-            def _():
-                crossed(z - j)
+            if ready is None:
+                @pl.when(z - j >= 0)
+                def _():
+                    crossed(z - j)
 
             @pl.when(z + j < depth)
             def _():
@@ -347,11 +358,10 @@
 
 
 def layer_kernel(depth, chips, experts,
-                 nope_ref, rope_ref, latent_ref, key_ref, latent_gain_ref, resid_ref, gain_ref, ids_ref, route_ref,
-                 table_hbm, kup_hbm, vup_hbm, proj_hbm, eg_hbm, eu_hbm, ed_hbm, sg_hbm, su_hbm, sd_hbm,
+                 latent_gain_ref, gain_ref, nope_hbm, rope_hbm, latent_hbm, key_hbm, resid_hbm, ids_hbm, route_hbm, table_hbm, kup_hbm, vup_hbm, proj_hbm, eg_hbm, eu_hbm, ed_hbm, sg_hbm, su_hbm, sd_hbm,
                  out_ref,
-                 table, kup, vup, proj_ref, eg, eu, ed, sg, su, sd, load_sem,
-                 lat, query, heads_ref, mixed, l_up, l_down, l_side, l_got, relay_out, relay_in,
+                 nope_ref, rope_ref, latent_ref, key_ref, resid_ref, ids_ref, route_ref, table, kup, vup, proj_ref, eg, eu, ed, sg, su, sd, load_sem,
+                 lat, query, heads_ref, mixed, tops, sums, l_up, l_down, l_side, l_got, relay_out, relay_in,
                  part, sib, ysend, yrecv, sib_s, sib_r, y_s, y_r,
                  hid, shared, xbuf, up, down, side, got,
                  contrib, xr, upr, dnr, rx_s, rx_r, rz_s, up_r, dn_r):
@@ -365,8 +375,10 @@
     local_heads = head_cols // NOPE
     columns = pl.ds(pl.multiple_of(t * head_cols, head_cols), head_cols)
     loads = [pltpu.make_async_copy(src, dst, load_sem.at[i]) for i, (src, dst) in enumerate(
-        ((table_hbm.at[pl.ds(pl.multiple_of(me * rows, rows), rows)], table),
-         (kup_hbm.at[:, columns], kup), (vup_hbm.at[:, columns], vup), (proj_hbm, proj_ref),
+        ((latent_hbm, latent_ref), (key_hbm, key_ref),
+         (table_hbm.at[pl.ds(pl.multiple_of(me * rows, rows), rows)], table),
+         (nope_hbm, nope_ref), (rope_hbm, rope_ref), (ids_hbm, ids_ref), (route_hbm, route_ref),
+         (kup_hbm.at[:, columns], kup), (vup_hbm.at[:, columns], vup), (proj_hbm, proj_ref), (resid_hbm, resid_ref),
          (sg_hbm, sg), (su_hbm, su), (sd_hbm, sd), (eg_hbm.at[0], eg), (eu_hbm.at[0], eu), (ed_hbm.at[0], ed)))]
     for load in loads:
         load.start()
@@ -374,14 +386,16 @@
     peers = [lax.rem(t + 2 * d, 2 * chips) for d in range(1, chips)]
     greet(z, depth, me, [sibling] + peers)
 
+    loads[0].wait()
     wide = latent_ref[...].astype(F32)
     factor = lax.rsqrt(jnp.mean(wide * wide, axis=-1, keepdims=True) + norm_eps)
     lat[me, :, :rank] = (wide * factor * latent_gain_ref[...].astype(F32)).astype(BF16)
-    loads[0].wait()
+    loads[1].wait()
+    loads[2].wait()
     cosine, sine = table[:, :ROPE], table[:, ROPE:]
     cosine = jnp.concatenate([cosine, cosine], axis=1)
     sine = jnp.concatenate([sine, sine], axis=1)
-    key = key_ref[...].astype(F32)
+    key = key_ref[...].astype(F32).T
     lat[me, :, rank:] = rotated(jnp.concatenate([key, key], axis=1), cosine, sine).astype(BF16)
 
     half_rows = rows // 2
@@ -397,34 +411,30 @@
 
     latents = Gather(lambda b, ch: half_view(b, c), 1, l_up, l_down, l_side, l_got, z, x, depth,
                      relay=lambda b, ch: relay_copy(b).start())
-    latents.start()
+    latents.start(0)
+    for load in loads[3:9]:
+        load.wait()
     lane = lax.broadcasted_iota(jnp.int32, (rows, LANES), 1)
     turned = rotated(rope_ref[...].astype(F32), cosine, sine)
     for h in range(local_heads):
         query[h, :, :NOPE] = nope_ref[:, h * NOPE:(h + 1) * NOPE]
         query[h, :, NOPE:] = jnp.where(lane // ROPE == h, turned, 0.0).astype(BF16)
-    lane = lax.broadcasted_iota(jnp.int32, (tokens, LANES), 1)
-    dense = jnp.zeros((tokens, LANES), F32)
-    for k in range(ids_ref.shape[1]):
-        dense = dense + jnp.where(lane % experts == ids_ref[:, k:k + 1], route_ref[:, k:k + 1], 0.0)
+    slot = lax.broadcasted_iota(jnp.int32, (LANES, tokens), 0)
+    dense = jnp.zeros((LANES, tokens), F32)
+    for k in range(ids_ref.shape[0]):
+        dense = dense + jnp.where(slot % experts == ids_ref[k:k + 1, :], route_ref[k:k + 1, :], 0.0)
     coarse = dense.astype(BF16).astype(F32)
-    terms = jnp.where(lane < experts, coarse, jnp.where(lane < 2 * experts, dense - coarse, 0.0))
-    xbuf[me, :, width:] = terms.astype(BF16)
-    loads[1].wait()
-    loads[2].wait()
+    terms = jnp.where(slot < experts, coarse, jnp.where(slot < 2 * experts, dense - coarse, 0.0))
+    xbuf[me, :, width:] = terms.T.astype(BF16)
     value_t = vup[...].astype(F32).T.astype(BF16)
     vup[...] = value_t
-    latents.run()
-    for block in range(2 * depth):
-        @pl.when(block != me)
-        def _():
-            arrived(half_view(block, 1 - c), relay_in.at[block])
-
     span = 2 * rows
     score_scale = 1.0 / math.sqrt(NOPE + ROPE)
     mixed[...] = jnp.zeros(mixed.shape, F32)
-
-    def attend(zz, state):
+    tops[...] = jnp.full(tops.shape, -1e30, F32)
+    sums[...] = jnp.zeros(sums.shape, F32)
+
+    def attend(zz):
         pair = lat[pl.ds(zz * 2, 2)].reshape(span, rank + LANES)
         keys = jnp.dot(pair[:, :rank], kup[...], preferred_element_type=F32).astype(BF16)
         values_t = lax.dot_general(
@@ -432,9 +442,8 @@
         key_pos = zz * span + lax.broadcasted_iota(jnp.int32, (span, rows), 0)
         query_pos = me * rows + lax.broadcasted_iota(jnp.int32, (span, rows), 1)
         allowed = key_pos <= query_pos
-        fresh = []
         for h in range(local_heads):
-            top, weight_sum = state[h]
+            top = tops[h]
             full = jnp.concatenate([keys[:, h * NOPE:(h + 1) * NOPE], pair[:, rank:]], axis=1)
             scores = lax.dot_general(
                 full, query[h], (((1,), (1,)), ((), ())), preferred_element_type=F32) * score_scale
@@ -442,62 +451,85 @@
             newest = jnp.maximum(top, jnp.max(scores, axis=0, keepdims=True))
             weights = jnp.exp(scores - newest)
             shrink = jnp.exp(top - newest)
-            weight_sum = weight_sum * shrink + jnp.sum(weights, axis=0, keepdims=True)
+            sums[h] = sums[h] * shrink + jnp.sum(weights, axis=0, keepdims=True)
             mixed[h] = mixed[h] * shrink + jnp.dot(
                 values_t[h * VDIM:(h + 1) * VDIM], weights.astype(BF16), preferred_element_type=F32)
-            fresh.append((newest, weight_sum))
-        return tuple(fresh)
-
-    first = tuple((jnp.full((1, rows), -1e30, F32), jnp.zeros((1, rows), F32)) for _ in range(local_heads))
-    folded = lax.fori_loop(0, z + 1, attend, first)
+            tops[h] = newest
+
+    def relayed(block):
+        arrived(half_view(block, 1 - c), relay_in.at[block])
+
+    def ready(zz, own):
+        across = zz * 2 + 1 - x
+        latents.take(across, 0)
+        relay_copy(across).start()
+        if not own:
+            relayed(zz * 2 + x)
+        relayed(across)
+        attend(zz)
+
+    latents.run(ready)
     for h in range(local_heads):
-        heads_ref[:, h * VDIM:(h + 1) * VDIM] = (mixed[h] / folded[h][1]).T.astype(BF16)
-    loads[3].wait()
+        heads_ref[:, h * VDIM:(h + 1) * VDIM] = (mixed[h] / sums[h]).T.astype(BF16)
+    loads[9].wait()
+    loads[10].wait()
 
     def project(block):
         mine = heads_ref[pl.ds(pl.multiple_of(block * tokens, tokens), tokens), :]
         return jnp.dot(mine, proj_ref[...], preferred_element_type=F32).astype(BF16)
 
-    def to_sibling(yy):
+    piece = tokens // CHUNKS
+
+    def to_sibling(yy, ch):
+        here = pl.ds(ch * piece, piece)
         return pltpu.make_async_remote_copy(
-            src_ref=part.at[yy], dst_ref=sib.at[yy], send_sem=sib_s.at[yy], recv_sem=sib_r.at[yy],
+            src_ref=part.at[yy, here], dst_ref=sib.at[yy, here], send_sem=sib_s.at[yy, ch], recv_sem=sib_r.at[yy, ch],
             device_id={"tp": sibling}, device_id_type=MESH)
 
-    def to_chip(d):
+    def to_chip(d, ch):
+        here = pl.ds(ch * piece, piece)
         return pltpu.make_async_remote_copy(
-            src_ref=ysend.at[d - 1], dst_ref=yrecv.at[d - 1], send_sem=y_s.at[d - 1], recv_sem=y_r.at[d - 1],
+            src_ref=ysend.at[d - 1, here], dst_ref=yrecv.at[d - 1, here],
+            send_sem=y_s.at[d - 1, ch], recv_sem=y_r.at[d - 1, ch],
             device_id={"tp": peers[d - 1]}, device_id_type=MESH)
 
+    def pair_sum(yy, mine, ch):
+        here = pl.ds(ch * piece, piece)
+        arrived(sib.at[yy, here], sib_r.at[yy, ch])
+        return mine[ch * piece:(ch + 1) * piece] + sib[yy, here].astype(F32)
+
     ahead = [lax.rem(y + d, chips) for d in range(1, chips)] + [y]
-    for yy in ahead:
+    for slot, yy in enumerate(ahead):
         part[yy] = project(yy * 2 + 1 - c)
-        to_sibling(yy).start()
+        for ch in range(CHUNKS):
+            to_sibling(yy, ch).start()
+        if slot < chips - 1:
+            ysend[slot] = project(yy * 2 + c)
     for d in range(1, chips):
-        yy = ahead[d - 1]
-        mine = project(yy * 2 + c).astype(F32)
-        arrived(sib.at[yy], sib_r.at[yy])
-        ysend[d - 1] = (mine + sib[yy].astype(F32)).astype(BF16)
-        to_chip(d).start()
-    total = project(y * 2 + c).astype(F32)
-    arrived(sib.at[y], sib_r.at[y])
-    total = total + sib[y].astype(F32)
-    for d in range(1, chips):
-        arrived(yrecv.at[d - 1], y_r.at[d - 1])
-        total = total + yrecv[d - 1].astype(F32)
-    hidden_one = (resid_ref[...].astype(F32) + total).astype(BF16)
-    hid[...] = hidden_one
-    wide = hidden_one.astype(F32)
-    factor = lax.rsqrt(jnp.mean(wide * wide, axis=-1, keepdims=True) + norm_eps)
-    xbuf[me, :, :width] = (wide * factor * gain_ref[...].astype(F32)).astype(BF16)
-
-    piece = tokens // CHUNKS
+        mine = ysend[d - 1].astype(F32)
+        for ch in range(CHUNKS):
+            ysend[d - 1, pl.ds(ch * piece, piece)] = pair_sum(ahead[d - 1], mine, ch).astype(BF16)
+            to_chip(d, ch).start()
+    mine = project(y * 2 + c).astype(F32)
+
     ring = Gather(lambda b, ch: xbuf.at[b, pl.ds(ch * piece, piece)], CHUNKS, up, down, side, got, z, x, depth)
-    ring.start()
-    for load in loads[4:7]:
+    for ch in range(CHUNKS):
+        here = pl.ds(ch * piece, piece)
+        total = pair_sum(y, mine, ch)
+        for d in range(1, chips):
+            arrived(yrecv.at[d - 1, here], y_r.at[d - 1, ch])
+            total = total + yrecv[d - 1, here].astype(F32)
+        hidden_one = (resid_ref[here].astype(F32) + total).astype(BF16)
+        hid[here] = hidden_one
+        wide = hidden_one.astype(F32)
+        factor = lax.rsqrt(jnp.mean(wide * wide, axis=-1, keepdims=True) + norm_eps)
+        xbuf[me, here, :width] = (wide * factor * gain_ref[...].astype(F32)).astype(BF16)
+        ring.start(ch)
+    for load in loads[11:14]:
         load.wait()
     shared[...] = gated(xbuf[me, :, :width], sg, su, sd)
     ring.run()
-    for load in loads[7:]:
+    for load in loads[14:]:
         load.wait()
 
     def cross(zz, ch):
@@ -584,14 +616,21 @@
         out_ref[here] = (hid[here].astype(F32) + routed.astype(F32) + shared[here].astype(F32)).astype(BF16)
 
     latents.finish()
+    for zz in range(depth):
+        @pl.when(zz > z)
+        def _():
+            relayed(zz * 2 + x)
+            relayed(zz * 2 + 1 - x)
+
     for block in range(2 * depth):
         @pl.when(block != me)
         def _():
             relay_copy(block).wait_send()
-    for yy in range(chips):
-        to_sibling(yy).wait_send()
-    for d in range(1, chips):
-        to_chip(d).wait_send()
+    for ch in range(CHUNKS):
+        for yy in range(chips):
+            to_sibling(yy, ch).wait_send()
+        for d in range(1, chips):
+            to_chip(d, ch).wait_send()
     ring.finish()
     for zz in range(depth):
         for ch in range(CHUNKS):
@@ -624,13 +663,16 @@
         return pltpu.VMEM(shape, BF16)
 
     scratch = [
+        buf(*query_nope.shape), buf(*query_rope.shape), buf(rows, rank), buf(ROPE, rows), buf(*block),
+        pltpu.VMEM(expert_ids.shape[::-1], jnp.int32), pltpu.VMEM(expert_ids.shape[::-1], F32),
         pltpu.VMEM((rows, 2 * ROPE), F32), buf(rank, head_cols), buf(rank, head_cols), buf(head_cols, width),
-        buf(width, ff), buf(width, ff), buf(ff, width), buf(width, ff), buf(width, ff), buf(ff, width), dma((10,)),
+        buf(width, ff), buf(width, ff), buf(ff, width), buf(width, ff), buf(width, ff), buf(ff, width), dma((17,)),
         buf(sp, rows, rank + LANES), buf(head_cols // NOPE, rows, NOPE + LANES), buf(rows, head_cols),
         pltpu.VMEM((head_cols // VDIM, VDIM, rows), F32),
+        pltpu.VMEM((head_cols // NOPE, 1, rows), F32), pltpu.VMEM((head_cols // NOPE, 1, rows), F32),
         dma((depth, 1)), dma((depth, 1)), dma((depth, 1)), dma((sp, 1)), dma((sp,)), dma((sp,)),
         buf(chips, *block), buf(chips, *block), buf(chips - 1, *block), buf(chips - 1, *block),
-        dma((chips,)), dma((chips,)), dma((chips - 1,)), dma((chips - 1,)),
+        dma((chips, CHUNKS)), dma((chips, CHUNKS)), dma((chips - 1, CHUNKS)), dma((chips - 1, CHUNKS)),
         buf(*block), buf(*block), buf(sp, tokens, width + LANES),
         dma((depth, CHUNKS)), dma((depth, CHUNKS)), dma((depth, CHUNKS)), dma((sp, CHUNKS)),
         buf(depth, 2, *block), buf(depth, *block), buf(depth, *block), buf(depth, *block),
@@ -638,14 +680,14 @@
     return pl.pallas_call(
         functools.partial(layer_kernel, depth, chips, sp),
         out_shape=jax.ShapeDtypeStruct(block, BF16),
-        in_specs=[vmem] * 9 + [hbm] * 10,
+        in_specs=[vmem] * 2 + [hbm] * 17,
         out_specs=vmem,
         scratch_shapes=scratch,
         compiler_params=pltpu.CompilerParams(
-            collective_id=0, has_side_effects=True, vmem_limit_bytes=48 * 1024 * 1024),
+            collective_id=0, has_side_effects=True, vmem_limit_bytes=67043328),
         name="layer",
-    )(query_nope, query_rope, latent, key_rope, latent_gain.reshape(1, -1), residual, ffn_gain.reshape(1, -1),
-      expert_ids, route_weights, table, key_up, value_up, out_proj,
+    )(latent_gain, ffn_gain, query_nope, query_rope, latent, key_rope.T, residual,
+      expert_ids.T, route_weights.T, table, key_up, value_up, out_proj,
       expert_gate, expert_up, expert_down, shared_gate, shared_up, shared_down)
 
 

time: 105 us -> 89 us (0.85)
  local copies, waits for them, and re-layouts: 14 us -> 1.67 us
  Pallas kernels: 90.6 us -> 87.1 us
    unnamed x22 -> x1, local copies, waits for them, and re-layouts: 12.6 us -> 1.67 us
    pallas_call x1, Pallas kernels: 90.6 us -> 87.1 us  [line_body(): pl.pallas_call(functools.partial(layer_kernel, depth, chips, sp), out_sha...]
    reshape x2 -> x0, local copies, waits for them, and re-layouts: 1.35 us -> none  [the longest x1 0.69 us: line_body(): ffn_gain.reshape(1, -1)]
where the time goes in v3:
time: 89 us; the launch traced here: 88.8 us
  Pallas kernels  87.1 us (98%)
  local copies, waits for them, and re-layouts  1.67 us (2%)
    pallas_call x1, Pallas kernels, line_body(): pl.pallas_call(functools.partial(layer_kernel, depth, chips, sp), out_sha...  87.1 us

profile of v3, /device:TPU:0, one launch (start us, length us, event | category | flops | bytes accessed | tf_op | source)
XLA Modules:
  0.0 88.8 jit_solution(9276728257007187258)
XLA Ops:
  0.0 87.1 %layer.1 = bf16[64,2048]{1,0:T(8,128)(2,1)} custom-call(bf16[256]{0:T(256)(128)(2,1)} %latent_gain_ref.1, bf16[2048]{0:T(1024)(128)(2,1)} %gain_ref.1, bf16[256,256]{1,0:T(8,128)(2,1)} %nope_hbm.1, bf16[256,128]{1,0:T(8,128)(2,1)} %rope_hbm.1, bf16[256,256]{1,0:T(8,128)(2,1)} %latent_hbm.1, bf16[64,256]{1,0:T(8,128)(2,1)} %bitcast.3, ...), custom_call_target="tpu_custom_call" | custom-call | tf_op jit(solution)/shard_map/layer/pallas_call | solution.py:680
  87.1 1.7 %copy.21 = bf16[64,2048]{1,0:T(8,128)(2,1)} copy(bf16[64,2048]{1,0:T(8,128)(2,1)} %layer.1) | data formatting | bytes 524288

commit v4 on v3

--- a/solution.py
+++ b/solution.py
@@ -347,7 +347,7 @@
     return jnp.dot(hidden, down[...], preferred_element_type=F32).astype(BF16)
 
 
-CHUNKS = 2
+CHUNKS = 4
 
 
 def rotated(values, cosine, sine):

time: 89 us -> 98 us (1.10)
  Pallas kernels: 87.1 us -> 96.1 us
    pallas_call x1, Pallas kernels: 87.1 us -> 96.1 us  [line_body(): pl.pallas_call(functools.partial(layer_kernel, depth, chips, sp), out_sha...]
where the time goes in v4:
time: 98 us; the launch traced here: 97.8 us
  Pallas kernels  96.1 us (98%)
  local copies, waits for them, and re-layouts  1.67 us (2%)
    pallas_call x1, Pallas kernels, line_body(): pl.pallas_call(functools.partial(layer_kernel, depth, chips, sp), out_sha...  96.1 us

profile of v4, /device:TPU:0, one launch (start us, length us, event | category | flops | bytes accessed | tf_op | source)
XLA Modules:
  0.0 97.8 jit_solution(68012814309572678)
XLA Ops:
  0.0 96.1 %layer.1 = bf16[64,2048]{1,0:T(8,128)(2,1)} custom-call(bf16[256]{0:T(256)(128)(2,1)} %latent_gain_ref.1, bf16[2048]{0:T(1024)(128)(2,1)} %gain_ref.1, bf16[256,256]{1,0:T(8,128)(2,1)} %nope_hbm.1, bf16[256,128]{1,0:T(8,128)(2,1)} %rope_hbm.1, bf16[256,256]{1,0:T(8,128)(2,1)} %latent_hbm.1, bf16[64,256]{1,0:T(8,128)(2,1)} %bitcast.3, ...), custom_call_target="tpu_custom_call" | custom-call | tf_op jit(solution)/shard_map/layer/pallas_call | solution.py:680
  96.1 1.7 %copy.21 = bf16[64,2048]{1,0:T(8,128)(2,1)} copy(bf16[64,2048]{1,0:T(8,128)(2,1)} %layer.1) | data formatting | bytes 524288

commit v5 on v3

--- a/solution.py
+++ b/solution.py
@@ -234,8 +234,9 @@
 
 
 class Gather:
-    def __init__(self, view, chunks, up, down, side, got, z, x, depth, relay=None):
+    def __init__(self, view, whole, chunks, up, down, side, got, z, x, depth, relay=None):
         self.view, self.up, self.down, self.side, self.got = view, up, down, side, got
+        self.whole = whole
         self.z, self.x, self.depth, self.chunks = z, x, depth, chunks
         self.relay = relay if relay is not None else (lambda block, ch: None)
         self.me = z * 2 + x
@@ -251,8 +252,14 @@
     def send_down(self, zz, ch):
         return self.copy(zz * 2 + self.x, ch, self.down.at[zz, ch], self.me - 2)
 
-    def send_side(self, zz, ch):
-        return self.copy(zz * 2 + self.x, ch, self.side.at[zz, ch], self.z * 2 + 1 - self.x)
+    def send_side(self, zz):
+        block = zz * 2 + self.x
+        return pltpu.make_async_remote_copy(
+            src_ref=self.whole(block), dst_ref=self.whole(block), send_sem=self.side.at[zz, 0],
+            recv_sem=self.got.at[block, 0], device_id={"sp": self.z * 2 + 1 - self.x}, device_id_type=MESH)
+
+    def take_side(self, block):
+        arrived(self.whole(block), self.got.at[block, 0])
 
     def take(self, block, ch):
         arrived(self.view(block, ch), self.got.at[block, ch])
@@ -268,7 +275,8 @@
         def _():
             self.send_down(z, ch).start()
 
-        self.send_side(z, ch).start()
+        if ch == self.chunks - 1:
+            self.send_side(z).start()
 
     def run(self, ready=None):
         z, x, depth = self.z, self.x, self.depth
@@ -283,7 +291,8 @@
                     def _():
                         self.send_up(zz, ch).start()
 
-                    self.send_side(zz, ch).start()
+                    if ch == self.chunks - 1:
+                        self.send_side(zz).start()
                     self.relay(zz * 2 + x, ch)
 
                 @pl.when(z + j < depth)
@@ -295,7 +304,8 @@
                     def _():
                         self.send_down(zz, ch).start()
 
-                    self.send_side(zz, ch).start()
+                    if ch == self.chunks - 1:
+                        self.send_side(zz).start()
                     self.relay(zz * 2 + x, ch)
 
             if ready is not None:
@@ -305,9 +315,8 @@
 
         def crossed(zz):
             block = zz * 2 + 1 - x
-            for ch in range(self.chunks):
-                self.take(block, ch)
-                self.relay(block, ch)
+            self.take_side(block)
+            self.relay(block, 0)
 
         if ready is not None:
             @pl.when(z - depth + 1 >= 0)
@@ -337,7 +346,7 @@
                 def _():
                     self.send_down(zz, ch).wait_send()
 
-                self.send_side(zz, ch).wait_send()
+            self.send_side(zz).wait_send()
 
 
 def gated(rows, gate, up, down):
@@ -409,7 +418,7 @@
             send_sem=relay_out.at[block], recv_sem=relay_in.at[block],
             device_id={"tp": sibling}, device_id_type=MESH)
 
-    latents = Gather(lambda b, ch: half_view(b, c), 1, l_up, l_down, l_side, l_got, z, x, depth,
+    latents = Gather(lambda b, ch: half_view(b, c), lambda b: half_view(b, c), 1, l_up, l_down, l_side, l_got, z, x, depth,
                      relay=lambda b, ch: relay_copy(b).start())
     latents.start(0)
     for load in loads[3:9]:
@@ -461,7 +470,7 @@
 
     def ready(zz, own):
         across = zz * 2 + 1 - x
-        latents.take(across, 0)
+        latents.take_side(across)
         relay_copy(across).start()
         if not own:
             relayed(zz * 2 + x)
@@ -512,7 +521,8 @@
             to_chip(d, ch).start()
     mine = project(y * 2 + c).astype(F32)
 
-    ring = Gather(lambda b, ch: xbuf.at[b, pl.ds(ch * piece, piece)], CHUNKS, up, down, side, got, z, x, depth)
+    ring = Gather(lambda b, ch: xbuf.at[b, pl.ds(ch * piece, piece)], lambda b: xbuf.at[b], CHUNKS,
+                  up, down, side, got, z, x, depth)
     for ch in range(CHUNKS):
         here = pl.ds(ch * piece, piece)
         total = pair_sum(y, mine, ch)
@@ -532,10 +542,10 @@
     for load in loads[14:]:
         load.wait()
 
-    def cross(zz, ch):
+    def cross(zz):
         return pltpu.make_async_remote_copy(
-            src_ref=contrib.at[zz, 1 - x, pl.ds(ch * piece, piece)], dst_ref=xr.at[zz, pl.ds(ch * piece, piece)],
-            send_sem=rx_s.at[zz, ch], recv_sem=rx_r.at[zz, ch],
+            src_ref=contrib.at[zz, 1 - x], dst_ref=xr.at[zz],
+            send_sem=rx_s.at[zz, 0], recv_sem=rx_r.at[zz, 0],
             device_id={"sp": z * 2 + 1 - x}, device_id_type=MESH)
 
     high = (z >= depth // 2).astype(jnp.int32)
@@ -551,8 +561,7 @@
         weight = jnp.sum(jnp.where((lane == me) | (lane == me + experts), routes, 0.0), axis=1, keepdims=True)
         answer = gated(pair[:, :width], eg, eu, ed).astype(F32) * weight
         contrib[zz] = answer.astype(BF16).reshape(2, tokens, width)
-        for ch in range(CHUNKS):
-            cross(zz, ch).start()
+        cross(zz).start()
         return carry
 
     lax.fori_loop(0, depth, expert_step, 0)
@@ -565,7 +574,8 @@
 
     def local_sum(dst, ch):
         here = pl.ds(ch * piece, piece)
-        arrived(xr.at[dst, here], rx_r.at[dst, ch])
+        if ch == 0:
+            arrived(xr.at[dst], rx_r.at[dst, 0])
         return contrib[dst, x, here].astype(F32) + xr[dst, here].astype(F32)
 
     def hop(dst, ch, landing, recv, at_end, to):
@@ -633,9 +643,8 @@
             to_chip(d, ch).wait_send()
     ring.finish()
     for zz in range(depth):
+        cross(zz).wait_send()
         for ch in range(CHUNKS):
-            cross(zz, ch).wait_send()
-
             @pl.when(zz != z)
             def _():
                 arrived(contrib.at[zz, x, pl.ds(ch * piece, piece)], rz_s.at[zz, ch])

time: 89 us -> 93.7 us (1.053)
  Pallas kernels: 87.1 us -> 91.8 us
    pallas_call x1, Pallas kernels: 87.1 us -> 91.8 us  [line_body(): pl.pallas_call(functools.partial(layer_kernel, depth, chips, sp), out_sha...]
where the time goes in v5:
time: 93.7 us; the launch traced here: 93.5 us
  Pallas kernels  91.8 us (98%)
  local copies, waits for them, and re-layouts  1.67 us (2%)
    pallas_call x1, Pallas kernels, line_body(): pl.pallas_call(functools.partial(layer_kernel, depth, chips, sp), out_sha...  91.8 us

profile of v5, /device:TPU:0, one launch (start us, length us, event | category | flops | bytes accessed | tf_op | source)
XLA Modules:
  0.0 93.5 jit_solution(9006320454148173053)
XLA Ops:
  0.0 91.8 %layer.1 = bf16[64,2048]{1,0:T(8,128)(2,1)} custom-call(bf16[256]{0:T(256)(128)(2,1)} %latent_gain_ref.1, bf16[2048]{0:T(1024)(128)(2,1)} %gain_ref.1, bf16[256,256]{1,0:T(8,128)(2,1)} %nope_hbm.1, bf16[256,128]{1,0:T(8,128)(2,1)} %rope_hbm.1, bf16[256,256]{1,0:T(8,128)(2,1)} %latent_hbm.1, bf16[64,256]{1,0:T(8,128)(2,1)} %bitcast.3, ...), custom_call_target="tpu_custom_call" | custom-call | tf_op jit(solution)/shard_map/layer/pallas_call | solution.py:689
  91.8 1.7 %copy.21 = bf16[64,2048]{1,0:T(8,128)(2,1)} copy(bf16[64,2048]{1,0:T(8,128)(2,1)} %layer.1) | data formatting | bytes 524288
